TPU v7x, 32 devices: a whole 2x2x4 slice. The times are simulated.
32 devices in a mesh: sp: 8 (over z, x), tp: 4 (over y, core).
Axes of the slice: x: 2, y: 2, z: 4, core: 2. Of those that a mesh axis runs over, the one named last changes fastest.
Arguments:
- q_first: bfloat16 [1536, 512], P('sp', 'tp'), may hold values from -6 to 6
- k_first: bfloat16 [1536, 512], P('sp', 'tp'), may hold values from -6 to 6
- q_second: bfloat16 [1536, 512], P('sp', 'tp'), may hold values from -6 to 6
- k_second: bfloat16 [1536, 512], P('sp', 'tp'), may hold values from -6 to 6
- values: bfloat16 [1536, 1024], P('sp', 'tp'), may hold values from -6 to 6
- lambdas: float32 [8], P('tp'), may hold values from 0.3 to 0.8
- head_gain: float32 [128], replicated, may hold values from 0.1 to 1.9
- out_weight: bfloat16 [1024, 2048], P('tp'), may hold values from -0.1875 to 0.1875
- residual_in: bfloat16 [1536, 2048], P('sp'), may hold values from -6 to 6
- mix_gain: float32 [2048], replicated, may hold values from 0.1 to 1.9
- gate_weight: bfloat16 [2048, 5632], P('sp', 'tp'), may hold values from -0.125 to 0.125
- up_weight: bfloat16 [2048, 5632], P('sp', 'tp'), may hold values from -0.125 to 0.125
- gate_taps: float32 [3, 5632], P(None, 'tp'), may hold values from -3.5 to 3.5
- up_taps: float32 [3, 5632], P(None, 'tp'), may hold values from -3.5 to 3.5
- down_weight: bfloat16 [5632, 2048], P('tp'), may hold values from -0.078125 to 0.078125
Outputs:
- mixed: bfloat16 [1536, 2048], P(('sp', 'tp'))
All inputs are finite; a program needn't handle non-finite values.
Results may differ from a plain program's by a relative error of at most 0.017.
Values may be sent and summed in bfloat16 or wider, within the bound.
A program may use at most 128 MiB of HBM per device.

v0:
```python
import functools

import jax
import jax.numpy as jnp
from jax import lax
from jax.experimental import pallas as pl
from jax.experimental.pallas import tpu as pltpu
from jax.sharding import PartitionSpec as P

norm_eps = 1e-06
far_below = -1e30
halo = 16
lanes = 2
team = 2
f32 = jnp.float32
bf16 = jnp.bfloat16


def rms_scale(field, gain):
    return field * lax.rsqrt(jnp.mean(field * field, axis=-1, keepdims=True) + norm_eps) * gain


def layer(
    sp_count,
    tp_count,
    q_a,
    k_a,
    q_b,
    k_b,
    vals,
    lambdas,
    head_gain,
    out_weight,
    residual,
    mix_gain,
    gate_weight,
    up_weight,
    gate_taps,
    up_taps,
    down_weight,
    out,
    kv,
    w_own,
    w,
    down,
    out_w,
    res,
    heads,
    part_out,
    part_in,
    stream,
    ffn,
    acc,
    hidden,
    pair_out,
    pair_in,
    last_out,
    last_in,
    local,
    kvz_send,
    kvz_recv,
    kvx_send,
    kvx_recv,
    wz_send,
    wz_recv,
    wx_send,
    wx_recv,
    rs_send,
    rs_recv,
    ag_send,
    ag_recv,
    halo_send,
    halo_recv,
    pair_send,
    pair_recv,
    last_send,
    last_recv,
):
    s = lax.axis_index("sp")
    t = lax.axis_index("tp")
    x = lax.rem(s, lanes)
    z = s // lanes
    lines = sp_count // lanes
    mate = z * lanes + (1 - x)
    rows = q_a.shape[0]
    key_width = q_a.shape[1]
    value_width = vals.shape[1]
    head_count = lambdas.shape[0]
    head_dim = key_width // head_count
    value_dim = value_width // head_count
    part = rows // tp_count
    width = out.shape[1]
    w_rows = gate_weight.shape[0]
    ff = gate_weight.shape[1]
    taps = gate_taps.shape[0]
    piece = w.shape[2]
    shift = ff - piece
    g = lax.rem(z, team)
    partner = (z + 1 - 2 * g) * lanes + x
    slot_rows = halo + rows

    def columns(line):
        return pl.multiple_of(lax.rem(line, team) * shift, 128)


    def remote(src, dst, send, recv, sp, tp):
        return pltpu.make_async_remote_copy(
            src_ref=src,
            dst_ref=dst,
            send_sem=send,
            recv_sem=recv,
            device_id=(sp, tp),
            device_id_type=pl.DeviceIdType.MESH,
        )

    def kv_block(block):
        return kv.at[pl.ds(pl.multiple_of(block * rows, 16), rows)]

    def w_block(c, block):
        return w.at[c, pl.ds(pl.multiple_of(block * w_rows, 16), w_rows)]

    own = pl.ds(pl.multiple_of(s * rows, 16), rows)
    kv_loads = (
        pltpu.make_async_copy(k_a, kv.at[own, pl.ds(0, key_width)], local.at[0]),
        pltpu.make_async_copy(k_b, kv.at[own, pl.ds(key_width, key_width)], local.at[1]),
        pltpu.make_async_copy(vals, kv.at[own, pl.ds(2 * key_width, value_width)], local.at[2]),
    )
    w_loads = (
        pltpu.make_async_copy(gate_weight, w_own.at[0], local.at[3]),
        pltpu.make_async_copy(up_weight, w_own.at[1], local.at[4]),
        pltpu.make_async_copy(gate_weight.at[:, pl.ds(columns(z), piece)], w_block(0, s), local.at[8]),
        pltpu.make_async_copy(up_weight.at[:, pl.ds(columns(z), piece)], w_block(1, s), local.at[9]),
    )
    out_load = pltpu.make_async_copy(out_weight, out_w, local.at[5])
    res_load = pltpu.make_async_copy(
        residual.at[pl.ds(pl.multiple_of(t * part, 16), part)], res, local.at[6]
    )
    down_load = pltpu.make_async_copy(down_weight.at[pl.ds(columns(z), piece)], down, local.at[7])
    for load in kv_loads + w_loads + (out_load, res_load, down_load):
        load.start()

    barrier = pltpu.get_barrier_semaphore()

    @pl.loop(1, sp_count)
    def _(i):
        pl.semaphore_signal(
            barrier,
            inc=1,
            device_id=(lax.rem(s + i, sp_count), t),
            device_id_type=pl.DeviceIdType.MESH,
        )

    @pl.loop(1, tp_count)
    def _(i):
        pl.semaphore_signal(
            barrier,
            inc=1,
            device_id=(s, lax.rem(t + i, tp_count)),
            device_id_type=pl.DeviceIdType.MESH,
        )

    for i in range(1, tp_count):
        pl.semaphore_signal(
            barrier,
            inc=1,
            device_id=(partner, lax.rem(t + i, tp_count)),
            device_id_type=pl.DeviceIdType.MESH,
        )

    pl.semaphore_wait(barrier, sp_count + 2 * tp_count - 3)

    def kvz(line, to, index):
        block = kv_block(line * lanes + x)
        return remote(block, block, kvz_send.at[index], kvz_recv.at[line], to * lanes + x, t)

    def kvx(line, lane):
        block = kv_block(line * lanes + lane)
        return remote(block, block, kvx_send.at[line], kvx_recv.at[line], mate, t)

    def wz(c, line, to, index):
        block = w_block(c, line * lanes + x)
        source = w_own.at[c, :, pl.ds(columns(to), piece)]
        return remote(source, block, wz_send.at[c, index], wz_recv.at[c, line], to * lanes + x, t)

    def wx(c, line, lane):
        block = w_block(c, line * lanes + lane)
        return remote(block, block, wx_send.at[c, line], wx_recv.at[c, line], mate, t)

    for load in kv_loads:
        load.wait()

    @pl.loop(z + 1, lines)
    def _(to):
        kvz(z, to, to).start()

    kvx(z, x).start()
    for load in w_loads:
        load.wait()

    def send_weights(i):
        to = lax.rem(z + lines - i, lines)
        for c in range(2):
            wz(c, z, to, to).start()

    @pl.loop(1, lines - 1)
    def _(i):
        send_weights(i)

    @pl.loop(0, z)
    def _(i):
        line = z - 1 - i
        kvz(line, mate // lanes, line).wait_recv()
        kvx(line, x).start()

    for c in range(2):
        wx(c, z, x).start()

    scale = head_dim**-0.5
    column = lax.broadcasted_iota(jnp.int32, (rows, key_width), 1) // head_dim
    queries = [
        jnp.where(column == h, q[...], jnp.zeros((), bf16))
        for q in (q_a, q_b)
        for h in range(head_count)
    ]
    span = lanes * rows
    query_pos = s * rows + lax.broadcasted_iota(jnp.int32, (rows, span), 0)
    key_step = lax.broadcasted_iota(jnp.int32, (rows, span), 1)

    def attend(i, state):
        line = z - i
        kvx(line, 1 - x).wait_recv()
        keys_at = pl.ds(pl.multiple_of(line * span, 16), span)
        visible = line * span + key_step <= query_pos
        following = []
        for m in range(2):
            keys = kv[keys_at, pl.ds(m * key_width, key_width)]
            for h in range(head_count):
                peak, total, sums = state[m * head_count + h]
                value = kv[keys_at, pl.ds(2 * key_width + h * value_dim, value_dim)]
                scores = (
                    lax.dot_general(
                        queries[m * head_count + h],
                        keys,
                        (((1,), (1,)), ((), ())),
                        preferred_element_type=f32,
                    )
                    * scale
                )
                scores = jnp.where(visible, scores, far_below)
                new_peak = jnp.maximum(peak, jnp.max(scores, axis=-1, keepdims=True))
                fade = jnp.exp(peak - new_peak)
                expo = jnp.exp(scores - new_peak)
                total = total * fade + jnp.sum(expo, axis=-1, keepdims=True)
                sums = sums * fade + jnp.dot(expo.astype(bf16), value, preferred_element_type=f32)
                following.append((new_peak, total, sums))
        return tuple(following)

    start = tuple(
        (
            jnp.full((rows, 1), far_below, f32),
            jnp.zeros((rows, 1), f32),
            jnp.zeros((rows, value_dim), f32),
        )
        for _ in range(2 * head_count)
    )
    state = lax.fori_loop(0, z + 1, attend, start)
    for h in range(head_count):
        _, total_a, sums_a = state[h]
        _, total_b, sums_b = state[head_count + h]
        diff = sums_a / total_a - lambdas[h] * (sums_b / total_b)
        heads[:, h * value_dim : (h + 1) * value_dim] = rms_scale(diff, head_gain[...]).astype(bf16)

    def forward(i):
        line = lax.rem(z + i, lines)
        for c in range(2):
            wz(c, line, mate // lanes, line).wait_recv()
            wx(c, line, x).start()

    early = min(3, lines - 1)
    if early > 0:
        forward(1)

    out_load.wait()
    res_load.wait()
    stream[...] = res[...].astype(f32)

    def part_copy(i):
        to = lax.rem(t + i, tp_count)
        return remote(part_out.at[to], part_in.at[t], rs_send.at[to], rs_recv.at[t], s, to)

    for i in range(1, tp_count + 1):
        to = lax.rem(t + i, tp_count)
        product = jnp.dot(
            heads[pl.ds(pl.multiple_of(to * part, 16), part), :],
            out_w[...],
            preferred_element_type=f32,
        )
        if i < tp_count:
            part_out[to] = product.astype(bf16)
            part_copy(i).start()
        else:
            stream[...] += product
    for i in range(1, tp_count):
        source = lax.rem(t + i, tp_count)
        remote(
            part_out.at[source], part_in.at[source], rs_send.at[source], rs_recv.at[source], s, source
        ).wait_recv()
        stream[...] += part_in[source].astype(f32)

    def ffn_rows(slot, rank):
        return pl.ds(pl.multiple_of(slot * slot_rows + halo + rank * part, 16), part)

    ffn[ffn_rows(g, t), :] = rms_scale(stream[...], mix_gain[...]).astype(bf16)

    def team_copy(slot):
        rows_here = ffn.at[ffn_rows(slot, t)]
        return remote(rows_here, rows_here, ag_send.at[slot, t], ag_recv.at[slot, t], partner, t)

    def gather_copy(i, slot, rank):
        to = lax.rem(t + i, tp_count)
        rows_here = ffn.at[ffn_rows(slot, rank)]
        return remote(rows_here, rows_here, ag_send.at[slot, to], ag_recv.at[slot, rank], s, to)

    team_copy(g).start()
    send_weights(lines - 1)
    for i in range(1, tp_count):
        gather_copy(i, g, t).start()
    if early > 1:
        forward(2)
    for i in range(1, tp_count):
        gather_copy(i, g, lax.rem(t + i, tp_count)).wait_recv()

    after = lax.rem(s + 1, sp_count)
    after_line = after // lanes
    after_slot = lax.rem(after_line, team)
    after_other = (after_line + 1 - 2 * after_slot) * lanes + lax.rem(after, lanes)

    def halo_copy(which, target, slot):
        return remote(
            ffn.at[pl.ds(pl.multiple_of(g * slot_rows + rows, 16), halo)],
            ffn.at[pl.ds(pl.multiple_of(slot * slot_rows, 16), halo)],
            halo_send.at[which],
            halo_recv.at[slot],
            target,
            t,
        )

    @pl.when(s < sp_count - 1)
    def _():
        halo_copy(0, after, after_slot).start()

        halo_copy(1, after_other, after_slot).start()

    team_copy(1 - g).wait_recv()
    for i in range(1, tp_count):
        gather_copy(i, 1 - g, t).start()
    if early > 2:
        forward(3)

    for slot in range(team):
        block = (z - g + slot) * lanes + x

        @pl.when(block == 0)
        def _():
            ffn[slot * slot_rows : slot * slot_rows + halo, :] = jnp.zeros((halo, width), bf16)

        @pl.when(block > 0)
        def _():
            halo_copy(0, mate, slot).wait_recv()

    for i in range(1, tp_count):
        gather_copy(i, 1 - g, lax.rem(t + i, tp_count)).wait_recv()

    acc[...] = jnp.zeros_like(acc)

    def project(first, count):
        at = pl.ds(pl.multiple_of(first, 128), count)
        for c in range(2):
            acc[c] += jnp.dot(ffn[:, at], w[c, at, :], preferred_element_type=f32)

    line_rows = lanes * w_rows
    paced = line_rows % 128 == 0

    def arrive(i):
        line = lax.rem(z + i, lines)
        for c in range(2):
            wx(c, line, 1 - x).wait_recv()
        if paced:
            project(line * line_rows, line_rows)

    if paced:
        for i in range(early + 1, lines):
            arrive(i - early - 1)
            forward(i)

        @pl.loop(max(lines - early - 1, 0), lines)
        def _(i):
            arrive(i)
    else:

        @pl.loop(early + 1, lines)
        def _(i):
            forward(i)

        @pl.loop(0, lines)
        def _(i):
            arrive(i)

        @pl.loop(0, width // 256)
        def _(i):
            project(i * 256, 256)

    @pl.loop(0, piece // 128)
    def _(i):
        at = pl.ds(pl.multiple_of(i * 128, 128), 128)
        tap_at = pl.ds(pl.multiple_of(columns(z) + i * 128, 128), 128)
        fresh = i * 128 >= g * (piece - shift)
        for slot in range(team):
            made = []
            for c, tap in enumerate((gate_taps, up_taps)):
                total = None
                for k in range(taps):
                    first = slot * slot_rows + halo - taps + 1 + k
                    row = acc[c, pl.ds(first, rows), at].astype(bf16).astype(f32)
                    term = tap[pl.ds(k, 1), tap_at] * row
                    total = term if total is None else total + term
                made.append(total)
            value = made[0] / (1 + jnp.exp(-made[0])) * made[1]
            hidden[slot * rows : (slot + 1) * rows, at] = jnp.where(fresh, value, 0.0).astype(bf16)

    down_load.wait()
    chunk = last_out.shape[2]
    chunks = width // chunk
    pairs = tp_count // 2
    c_own = lax.rem(t, 2)
    k_own = t // 2

    def pair_rows(far, k):
        return pl.ds(pl.multiple_of((far * pairs + k) * part, 16), part)

    def pair_copy(n):
        return remote(
            pair_out.at[n, 1 - c_own],
            pair_in.at[n],
            pair_send.at[n],
            pair_recv.at[n],
            s,
            t + 1 - 2 * c_own,
        )

    def last_copy(n, far, k, source):
        return remote(
            last_out.at[n, pair_rows(far, k)],
            last_in.at[n, pair_rows(far, source)],
            last_send.at[n, far * pairs + k],
            last_recv.at[n, far * pairs + source],
            partner if far else s,
            2 * k + c_own,
        )

    for n in range(chunks + 1):
        if n < chunks:
            for far in (1, 0):
                slot = 1 - g if far else g
                product = jnp.dot(
                    hidden[pl.ds(pl.multiple_of(slot * rows, 16), rows), :],
                    down[:, n * chunk : (n + 1) * chunk],
                    preferred_element_type=f32,
                ).astype(bf16)
                for r in range(tp_count):
                    first = (far * pairs + r // 2) * part
                    pair_out[n, r % 2, first : first + part] = product[r * part : (r + 1) * part]
            pair_copy(n).start()
        if n > 0:
            pair_copy(n - 1).wait_recv()
            both = pair_out[n - 1, c_own].astype(f32) + pair_in[n - 1].astype(f32)
            last_out[n - 1] = both.astype(bf16)
            for far in (1, 0):
                for i in range(1 - far, pairs):
                    last_copy(n - 1, far, lax.rem(k_own + i, pairs), k_own).start()
    for n in range(chunks):
        at = slice(n * chunk, (n + 1) * chunk)
        total = stream[:, at] + last_out[n, pair_rows(0, k_own), :].astype(f32)
        for far in (0, 1):
            for i in range(1 - far, pairs):
                source = lax.rem(k_own + i, pairs)
                last_copy(n, far, source, source).wait_recv()
                total = total + last_in[n, pair_rows(far, source), :].astype(f32)
        out[:, at] = total.astype(bf16)

    @pl.loop(z + 1, lines)
    def _(to):
        kvz(z, to, to).wait_send()

    @pl.loop(0, z + 1)
    def _(line):
        kvx(line, x).wait_send()

    @pl.loop(1, lines)
    def _(i):
        to = lax.rem(z + i, lines)
        for c in range(2):
            wz(c, z, to, to).wait_send()

    @pl.loop(0, lines)
    def _(line):
        for c in range(2):
            wx(c, line, x).wait_send()

    team_copy(g).wait_send()
    for i in range(1, tp_count):
        part_copy(i).wait_send()
        for slot in range(team):
            gather_copy(i, slot, t).wait_send()
    for n in range(chunks):
        pair_copy(n).wait_send()
        for far in (0, 1):
            for i in range(1 - far, pairs):
                last_copy(n, far, lax.rem(k_own + i, pairs), k_own).wait_send()

    @pl.when(s < sp_count - 1)
    def _():
        halo_copy(0, after, after_slot).wait_send()

        halo_copy(1, after_other, after_slot).wait_send()


def shards(sp_count, tp_count, *args):
    (q_a, _, _, _, vals, lambdas, head_gain, out_weight, residual, mix_gain, gate, _, _, _, down) = args
    rows = q_a.shape[0]
    width = residual.shape[1]
    w_rows, ff = gate.shape
    part = rows // tp_count
    lines = sp_count // lanes
    chunk = 512 if width % 512 == 0 else width
    share = team * tp_count // 2 * part
    piece = -(-ff // (team * 128)) * 128
    args = list(args)
    args[6] = head_gain.reshape(1, -1)
    args[9] = mix_gain.reshape(1, -1)
    vmem = pl.BlockSpec(memory_space=pltpu.VMEM)
    hbm = pl.BlockSpec(memory_space=pl.ANY)
    smem = pl.BlockSpec(memory_space=pltpu.SMEM)
    dma = pltpu.SemaphoreType.DMA
    in_specs = [vmem, hbm, vmem, hbm, hbm, smem, vmem, hbm, hbm, vmem, hbm, hbm, vmem, vmem, hbm]
    return pl.pallas_call(
        functools.partial(layer, sp_count, tp_count),
        out_shape=jax.ShapeDtypeStruct((part, width), bf16),
        in_specs=in_specs,
        out_specs=vmem,
        scratch_shapes=[
            pltpu.VMEM((sp_count * rows, 2 * q_a.shape[1] + vals.shape[1]), bf16),
            pltpu.VMEM((2, w_rows, ff), bf16),
            pltpu.VMEM((2, sp_count * w_rows, piece), bf16),
            pltpu.VMEM((piece, width), bf16),
            pltpu.VMEM(out_weight.shape, bf16),
            pltpu.VMEM((part, width), bf16),
            pltpu.VMEM((rows, vals.shape[1]), bf16),
            pltpu.VMEM((tp_count, part, width), bf16),
            pltpu.VMEM((tp_count, part, width), bf16),
            pltpu.VMEM((part, width), f32),
            pltpu.VMEM((team * (halo + rows), width), bf16),
            pltpu.VMEM((2, team * (halo + rows), piece), f32),
            pltpu.VMEM((team * rows, piece), bf16),
            pltpu.VMEM((width // chunk, 2, share, chunk), bf16),
            pltpu.VMEM((width // chunk, share, chunk), bf16),
            pltpu.VMEM((width // chunk, share, chunk), bf16),
            pltpu.VMEM((width // chunk, share, chunk), bf16),
            dma((10,)),
            dma((lines,)),
            dma((lines,)),
            dma((lines,)),
            dma((lines,)),
            dma((2, lines)),
            dma((2, lines)),
            dma((2, lines)),
            dma((2, lines)),
            dma((tp_count,)),
            dma((tp_count,)),
            dma((team, tp_count)),
            dma((team, tp_count)),
            dma((2,)),
            dma((team,)),
            dma((width // chunk,)),
            dma((width // chunk,)),
            dma((width // chunk, team * tp_count // 2)),
            dma((width // chunk, team * tp_count // 2)),
        ],
        compiler_params=pltpu.CompilerParams(
            collective_id=0, has_side_effects=True, vmem_limit_bytes=60 * 1024 * 1024
        ),
    )(*args)


def solution(mesh):
    in_specs = (
        P("sp", "tp"),
        P("sp", "tp"),
        P("sp", "tp"),
        P("sp", "tp"),
        P("sp", "tp"),
        P("tp"),
        P(),
        P("tp", None),
        P("sp", None),
        P(),
        P("sp", "tp"),
        P("sp", "tp"),
        P(None, "tp"),
        P(None, "tp"),
        P("tp", None),
    )
    body = functools.partial(shards, mesh.shape["sp"], mesh.shape["tp"])
    return jax.shard_map(
        body, mesh=mesh, in_specs=in_specs, out_specs=P(("sp", "tp"), None), check_vma=False
    )
```

profile of v0, /device:TPU:17, one launch (start us, length us, event | category | flops | bytes accessed | tf_op | source)
XLA Modules:
  0.0 154.3 jit_solution(17463026762482345658)
XLA Ops:
  0.0 152.7 %shard_map.145 = bf16[48,2048]{1,0:T(8,128)(2,1)} custom-call(bf16[192,128]{1,0:T(8,128)(2,1)} %q_a.1, bf16[192,128]{1,0:T(8,128)(2,1)} %k_a.1, bf16[192,128]{1,0:T(8,128)(2,1)} %q_b.1, bf16[192,128]{1,0:T(8,128)(2,1)} %k_b.1, bf16[192,256]{1,0:T(8,128)(2,1)} %vals.1, f32[2]{0:T(128)} %lambdas.1, f32[1,128]{1,0:T(1,128)} %bitcast.3, ...), custom_call_target="tpu_custom_call" | custom-call | tf_op jit(solution)/shard_map/pallas_call | solution.py:546
  152.7 1.6 %copy.17 = bf16[48,2048]{1,0:T(8,128)(2,1)} copy(bf16[48,2048]{1,0:T(8,128)(2,1)} %shard_map.145) | data formatting | bytes 393216
where the time goes:
time: 155 us; the launch traced here: 154 us
  Pallas kernels  153 us (99%)
  local copies, waits for them, and re-layouts  1.62 us (1%)
    pallas_call x1, Pallas kernels, shards(): pl.pallas_call(functools.partial(layer, sp_count, tp_count), out_shape=ja...  153 us

commit v1 on v0

v1 whole, which is shorter than its diff:
```python
import functools

import jax
import jax.numpy as jnp
from jax import lax
from jax.experimental import pallas as pl
from jax.experimental.pallas import tpu as pltpu
from jax.sharding import PartitionSpec as P

norm_eps = 1e-06
far_below = -1e30
halo = 16
lanes = 2
f32 = jnp.float32
bf16 = jnp.bfloat16


def rms_scale(field, gain):
    return field * lax.rsqrt(jnp.mean(field * field, axis=-1, keepdims=True) + norm_eps) * gain


def layer(
    sp_count,
    tp_count,
    team,
    q_a,
    k_a,
    q_b,
    k_b,
    vals,
    lambdas,
    head_gain,
    out_weight,
    residual,
    mix_gain,
    gate_weight,
    up_weight,
    gate_taps,
    up_taps,
    down_weight,
    out,
    kv,
    w_own,
    w,
    down,
    out_w,
    res,
    heads,
    part_out,
    part_in,
    stream,
    ffn,
    acc,
    hidden,
    pair_out,
    pair_in,
    y_out,
    y_in,
    z_out,
    z_in,
    local,
    kvz_send,
    kvz_recv,
    kvx_send,
    kvx_recv,
    wz_send,
    wz_recv,
    wx_send,
    wx_recv,
    rs_send,
    rs_recv,
    ag_send,
    ag_recv,
    halo_send,
    halo_recv,
    pair_send,
    pair_recv,
    y_send,
    y_recv,
    z_send,
    z_recv,
    team_send,
    team_recv,
):
    s = lax.axis_index("sp")
    t = lax.axis_index("tp")
    x = lax.rem(s, lanes)
    z = s // lanes
    lines = sp_count // lanes
    mate = z * lanes + (1 - x)
    rows = q_a.shape[0]
    key_width = q_a.shape[1]
    value_width = vals.shape[1]
    head_count = lambdas.shape[0]
    head_dim = key_width // head_count
    value_dim = value_width // head_count
    part = rows // tp_count
    width = out.shape[1]
    w_rows = gate_weight.shape[0]
    ff = gate_weight.shape[1]
    taps = gate_taps.shape[0]
    piece = w.shape[2]
    fresh = ff - (team - 1) * piece
    g = lax.rem(z, team)
    base = z - g
    slot_rows = halo + rows

    def member(slot):
        return (base + slot) * lanes + x

    def columns(line):
        return pl.multiple_of(jnp.minimum(lax.rem(line, team) * piece, ff - piece), 128)

    def by_width(line, act):
        if fresh == piece:
            act(0)
        else:
            last = lax.rem(line, team) == team - 1

            @pl.when(last)
            def _():
                act(piece - fresh)

            @pl.when(jnp.logical_not(last))
            def _():
                act(0)

    def remote(src, dst, send, recv, sp, tp):
        return pltpu.make_async_remote_copy(
            src_ref=src,
            dst_ref=dst,
            send_sem=send,
            recv_sem=recv,
            device_id=(sp, tp),
            device_id_type=pl.DeviceIdType.MESH,
        )

    def kv_block(block):
        return kv.at[pl.ds(pl.multiple_of(block * rows, 16), rows)]

    def w_block(c, block, skip=0):
        at = pl.ds(pl.multiple_of(block * w_rows, 16), w_rows)
        return w.at[c, at, pl.ds(skip, piece - skip)]

    own = pl.ds(pl.multiple_of(s * rows, 16), rows)
    kv_loads = (
        pltpu.make_async_copy(k_a, kv.at[own, pl.ds(0, key_width)], local.at[0]),
        pltpu.make_async_copy(k_b, kv.at[own, pl.ds(key_width, key_width)], local.at[1]),
        pltpu.make_async_copy(vals, kv.at[own, pl.ds(2 * key_width, value_width)], local.at[2]),
    )
    w_loads = (
        pltpu.make_async_copy(gate_weight, w_own.at[0], local.at[3]),
        pltpu.make_async_copy(up_weight, w_own.at[1], local.at[4]),
        pltpu.make_async_copy(gate_weight.at[:, pl.ds(columns(z), piece)], w_block(0, s), local.at[8]),
        pltpu.make_async_copy(up_weight.at[:, pl.ds(columns(z), piece)], w_block(1, s), local.at[9]),
    )
    out_load = pltpu.make_async_copy(out_weight, out_w, local.at[5])
    res_load = pltpu.make_async_copy(
        residual.at[pl.ds(pl.multiple_of(t * part, 16), part)], res, local.at[6]
    )
    down_load = pltpu.make_async_copy(down_weight.at[pl.ds(columns(z), piece)], down, local.at[7])
    for load in kv_loads + w_loads + (out_load, res_load, down_load):
        load.start()

    barrier = pltpu.get_barrier_semaphore()

    @pl.loop(1, sp_count)
    def _(i):
        pl.semaphore_signal(
            barrier,
            inc=1,
            device_id=(lax.rem(s + i, sp_count), t),
            device_id_type=pl.DeviceIdType.MESH,
        )

    @pl.loop(1, tp_count)
    def _(i):
        pl.semaphore_signal(
            barrier,
            inc=1,
            device_id=(s, lax.rem(t + i, tp_count)),
            device_id_type=pl.DeviceIdType.MESH,
        )

    @pl.loop(1, team)
    def _(j):
        @pl.loop(1, tp_count)
        def _(i):
            pl.semaphore_signal(
                barrier,
                inc=1,
                device_id=(member(lax.rem(g + j, team)), lax.rem(t + i, tp_count)),
                device_id_type=pl.DeviceIdType.MESH,
            )

    pl.semaphore_wait(barrier, sp_count - 1 + team * (tp_count - 1))

    def kvz(line, to, index):
        block = kv_block(line * lanes + x)
        return remote(block, block, kvz_send.at[index], kvz_recv.at[line], to * lanes + x, t)

    def kvx(line, lane):
        block = kv_block(line * lanes + lane)
        return remote(block, block, kvx_send.at[line], kvx_recv.at[line], mate, t)

    def wz(c, line, to, index, skip):
        block = w_block(c, line * lanes + x, skip)
        at = pl.ds(pl.multiple_of(columns(to) + skip, 128), piece - skip)
        return remote(
            w_own.at[c, :, at], block, wz_send.at[c, index], wz_recv.at[c, line], to * lanes + x, t
        )

    def wx(c, line, lane, skip):
        block = w_block(c, line * lanes + lane, skip)
        return remote(block, block, wx_send.at[c, line], wx_recv.at[c, line], mate, t)

    for load in kv_loads:
        load.wait()

    @pl.loop(0, lines - 1 - z)
    def _(i):
        to = lines - 1 - i
        kvz(z, to, to).start()

    kvx(z, x).start()
    for load in w_loads:
        load.wait()

    def near(distance, act):
        for line, there in ((z + distance, z + distance < lines), (z - distance, z >= distance)):

            @pl.when(there)
            def _():
                act(line)

    def send_weights(to):
        def act(skip):
            for c in range(2):
                wz(c, z, to, to, skip).start()

        by_width(to, act)

    @pl.loop(1, lines)
    def _(distance):
        near(distance, send_weights)

    scale = head_dim**-0.5
    column = lax.broadcasted_iota(jnp.int32, (rows, key_width), 1) // head_dim
    queries = [
        jnp.where(column == h, q[...], jnp.zeros((), bf16))
        for q in (q_a, q_b)
        for h in range(head_count)
    ]
    span = lanes * rows
    query_pos = s * rows + lax.broadcasted_iota(jnp.int32, (rows, span), 0)
    key_step = lax.broadcasted_iota(jnp.int32, (rows, span), 1)

    def attend(i, state):
        line = z - i

        @pl.when(i < z)
        def _():
            kvz(line - 1, mate // lanes, line - 1).wait_recv()
            kvx(line - 1, x).start()

        @pl.when(i == jnp.maximum(z - 1, 0))
        def _():
            def act(skip):
                for c in range(2):
                    wx(c, z, x, skip).start()

            by_width(z, act)

        kvx(line, 1 - x).wait_recv()
        keys_at = pl.ds(pl.multiple_of(line * span, 16), span)
        visible = line * span + key_step <= query_pos
        following = []
        for m in range(2):
            keys = kv[keys_at, pl.ds(m * key_width, key_width)]
            for h in range(head_count):
                peak, total, sums = state[m * head_count + h]
                value = kv[keys_at, pl.ds(2 * key_width + h * value_dim, value_dim)]
                scores = (
                    lax.dot_general(
                        queries[m * head_count + h],
                        keys,
                        (((1,), (1,)), ((), ())),
                        preferred_element_type=f32,
                    )
                    * scale
                )
                scores = jnp.where(visible, scores, far_below)
                new_peak = jnp.maximum(peak, jnp.max(scores, axis=-1, keepdims=True))
                fade = jnp.exp(peak - new_peak)
                expo = jnp.exp(scores - new_peak)
                total = total * fade + jnp.sum(expo, axis=-1, keepdims=True)
                sums = sums * fade + jnp.dot(expo.astype(bf16), value, preferred_element_type=f32)
                following.append((new_peak, total, sums))
        return tuple(following)

    start = tuple(
        (
            jnp.full((rows, 1), far_below, f32),
            jnp.zeros((rows, 1), f32),
            jnp.zeros((rows, value_dim), f32),
        )
        for _ in range(2 * head_count)
    )
    state = lax.fori_loop(0, z + 1, attend, start)
    for h in range(head_count):
        _, total_a, sums_a = state[h]
        _, total_b, sums_b = state[head_count + h]
        diff = sums_a / total_a - lambdas[h] * (sums_b / total_b)
        heads[:, h * value_dim : (h + 1) * value_dim] = rms_scale(diff, head_gain[...]).astype(bf16)

    def forward(line):
        def act(skip):
            for c in range(2):
                wz(c, line, mate // lanes, line, skip).wait_recv()
                wx(c, line, x, skip).start()

        by_width(z, act)

    early = min(3, lines - 1)
    if early > 0:
        near(1, forward)

    out_load.wait()
    res_load.wait()
    stream[...] = res[...].astype(f32)

    def part_copy(i):
        to = lax.rem(t + i, tp_count)
        return remote(part_out.at[to], part_in.at[t], rs_send.at[to], rs_recv.at[t], s, to)

    for i in range(1, tp_count + 1):
        to = lax.rem(t + i, tp_count)
        product = jnp.dot(
            heads[pl.ds(pl.multiple_of(to * part, 16), part), :],
            out_w[...],
            preferred_element_type=f32,
        )
        if i < tp_count:
            part_out[to] = product.astype(bf16)
            part_copy(i).start()
        else:
            stream[...] += product
    for i in range(1, tp_count):
        source = lax.rem(t + i, tp_count)
        remote(
            part_out.at[source], part_in.at[source], rs_send.at[source], rs_recv.at[source], s, source
        ).wait_recv()
        stream[...] += part_in[source].astype(f32)

    def ffn_rows(slot, rank):
        return pl.ds(pl.multiple_of(slot * slot_rows + halo + rank * part, 16), part)

    ffn[ffn_rows(g, t), :] = rms_scale(stream[...], mix_gain[...]).astype(bf16)

    def team_copy(slot, to):
        rows_here = ffn.at[ffn_rows(slot, t)]
        return remote(rows_here, rows_here, team_send.at[to], team_recv.at[slot], member(to), t)

    def gather_copy(i, slot, rank):
        to = lax.rem(t + i, tp_count)
        rows_here = ffn.at[ffn_rows(slot, rank)]
        return remote(rows_here, rows_here, ag_send.at[slot, to], ag_recv.at[slot, rank], s, to)

    for i in range(1, team):
        team_copy(g, lax.rem(g + i, team)).start()
    for i in range(1, tp_count):
        gather_copy(i, g, t).start()
    if early > 1:
        near(2, forward)
    for i in range(1, tp_count):
        gather_copy(i, g, lax.rem(t + i, tp_count)).wait_recv()

    after = lax.rem(s + 1, sp_count)
    after_line = after // lanes
    after_slot = lax.rem(after_line, team)
    after_base = after_line - after_slot

    def halo_copy(which, slot):
        return remote(
            ffn.at[pl.ds(pl.multiple_of(g * slot_rows + rows, 16), halo)],
            ffn.at[pl.ds(pl.multiple_of(slot * slot_rows, 16), halo)],
            halo_send.at[which],
            halo_recv.at[slot],
            (after_base + which) * lanes + lax.rem(after, lanes),
            t,
        )

    @pl.when(s < sp_count - 1)
    def _():
        for which in range(team):
            halo_copy(which, after_slot).start()

    for slot in range(team):
        if slot == team - 1 and early > 2:
            near(3, forward)

        @pl.when(slot != g)
        def _():
            team_copy(slot, g).wait_recv()
            for i in range(1, tp_count):
                gather_copy(i, slot, t).start()

    @pl.loop(early + 1, lines)
    def _(distance):
        near(distance, forward)

    @pl.loop(0, lines)
    def _(line):
        def act(skip):
            for c in range(2):
                wx(c, line, 1 - x, skip).wait_recv()

        by_width(z, act)

    down_load.wait()
    pairs = tp_count // 2
    c_own = lax.rem(t, 2)
    k_own = t // 2
    chunk = 512 if width % 512 == 0 else width

    def slot_of(n):
        return lax.rem(g + 1 + n, team)

    def part_rows(k):
        return pl.ds(pl.multiple_of(k * part, 16), part)

    def pair_copy(n):
        return remote(
            pair_out.at[n, 1 - c_own],
            pair_in.at[n],
            pair_send.at[n],
            pair_recv.at[n],
            s,
            t + 1 - 2 * c_own,
        )

    def y_copy(n, k, source):
        return remote(
            y_out.at[n, k],
            y_in.at[n, source],
            y_send.at[n, k],
            y_recv.at[n, source],
            s,
            2 * k + c_own,
        )

    def z_copy(n, source):
        return remote(
            z_out.at[n], z_in.at[source], z_send.at[n], z_recv.at[source], member(slot_of(n)), t
        )

    def compute(n):
        slot = slot_of(n)

        @pl.when(slot != g)
        def _():
            for i in range(1, tp_count):
                gather_copy(i, slot, lax.rem(t + i, tp_count)).wait_recv()

        block = member(slot)
        halo_rows = pl.ds(pl.multiple_of(slot * slot_rows, 16), halo)

        @pl.when(block == 0)
        def _():
            ffn[halo_rows, :] = jnp.zeros((halo, width), bf16)

        @pl.when(block > 0)
        def _():
            halo_copy(0, slot).wait_recv()

        rows_at = pl.ds(pl.multiple_of(slot * slot_rows, 16), slot_rows)
        for c in range(2):
            acc[c] = jnp.dot(ffn[rows_at, :], w[c], preferred_element_type=f32)
        for i in range(piece // 128):
            at = slice(i * 128, (i + 1) * 128)
            tap_at = pl.ds(pl.multiple_of(columns(z) + i * 128, 128), 128)
            made = []
            for c, tap in enumerate((gate_taps, up_taps)):
                total = None
                for k in range(taps):
                    first = halo - taps + 1 + k
                    row = acc[c, first : first + rows, at].astype(bf16).astype(f32)
                    term = tap[pl.ds(k, 1), tap_at] * row
                    total = term if total is None else total + term
                made.append(total)
            value = made[0] / (1 + jnp.exp(-made[0])) * made[1]
            if (i + 1) * 128 <= piece - fresh:
                value = jnp.where(g < team - 1, value, 0.0)
            hidden[:, at] = value.astype(bf16)
        for i in range(width // chunk):
            at = slice(i * chunk, (i + 1) * chunk)
            product = jnp.dot(hidden[...], down[:, at], preferred_element_type=f32).astype(bf16)
            for r in range(tp_count):
                first = (r // 2) * part
                pair_out[n, r % 2, first : first + part, at] = product[r * part : (r + 1) * part]
        pair_copy(n).start()

    def pair_sum(n, k):
        mine = pair_out[n, c_own, part_rows(k), :].astype(f32)
        return mine + pair_in[n, part_rows(k), :].astype(f32)

    def across(n):
        pair_copy(n).wait_recv()
        for i in range(1, pairs):
            k = lax.rem(k_own + i, pairs)
            y_out[n, k] = pair_sum(n, k).astype(bf16)
            y_copy(n, k, k_own).start()

    def along(n):
        total = pair_sum(n, k_own)
        for i in range(1, pairs):
            k = lax.rem(k_own + i, pairs)
            y_copy(n, k, k).wait_recv()
            total = total + y_in[n, k].astype(f32)
        if n < team - 1:
            z_out[n] = total.astype(bf16)
            z_copy(n, g).start()
        else:
            stream[...] += total

    for n in range(team + 2):
        if n < team:
            compute(n)
        if 0 < n <= team:
            across(n - 1)
        if n > 1:
            along(n - 2)
    for n in range(team - 1):
        source = slot_of(n)
        z_copy(n, source).wait_recv()
        stream[...] += z_in[source].astype(f32)
    out[...] = stream[...].astype(bf16)

    @pl.loop(z + 1, lines)
    def _(to):
        kvz(z, to, to).wait_send()

    @pl.loop(0, z + 1)
    def _(line):
        kvx(line, x).wait_send()

    @pl.loop(1, lines)
    def _(i):
        to = lax.rem(z + i, lines)

        def act(skip):
            for c in range(2):
                wz(c, z, to, to, skip).wait_send()

        by_width(to, act)

    @pl.loop(0, lines)
    def _(line):
        def act(skip):
            for c in range(2):
                wx(c, line, x, skip).wait_send()

        by_width(z, act)

    for i in range(1, team):
        team_copy(g, lax.rem(g + i, team)).wait_send()
    for i in range(1, tp_count):
        part_copy(i).wait_send()
        for slot in range(team):
            gather_copy(i, slot, t).wait_send()
    for n in range(team):
        pair_copy(n).wait_send()
        for i in range(1, pairs):
            y_copy(n, lax.rem(k_own + i, pairs), k_own).wait_send()
        if n < team - 1:
            z_copy(n, g).wait_send()

    @pl.when(s < sp_count - 1)
    def _():
        for which in range(team):
            halo_copy(which, after_slot).wait_send()


def shards(sp_count, tp_count, *args):
    (q_a, _, _, _, vals, lambdas, head_gain, out_weight, residual, mix_gain, gate, _, _, _, down) = args
    rows = q_a.shape[0]
    width = residual.shape[1]
    w_rows, ff = gate.shape
    part = rows // tp_count
    lines = sp_count // lanes
    team = next(n for n in (4, 2, 1) if lines % n == 0)
    pairs = tp_count // 2
    piece = -(-ff // (team * 128)) * 128
    args = list(args)
    args[6] = head_gain.reshape(1, -1)
    args[9] = mix_gain.reshape(1, -1)
    vmem = pl.BlockSpec(memory_space=pltpu.VMEM)
    hbm = pl.BlockSpec(memory_space=pl.ANY)
    smem = pl.BlockSpec(memory_space=pltpu.SMEM)
    dma = pltpu.SemaphoreType.DMA
    in_specs = [vmem, hbm, vmem, hbm, hbm, smem, vmem, hbm, hbm, vmem, hbm, hbm, vmem, vmem, hbm]
    return pl.pallas_call(
        functools.partial(layer, sp_count, tp_count, team),
        out_shape=jax.ShapeDtypeStruct((part, width), bf16),
        in_specs=in_specs,
        out_specs=vmem,
        scratch_shapes=[
            pltpu.VMEM((sp_count * rows, 2 * q_a.shape[1] + vals.shape[1]), bf16),
            pltpu.VMEM((2, w_rows, ff), bf16),
            pltpu.VMEM((2, sp_count * w_rows, piece), bf16),
            pltpu.VMEM((piece, width), bf16),
            pltpu.VMEM(out_weight.shape, bf16),
            pltpu.VMEM((part, width), bf16),
            pltpu.VMEM((rows, vals.shape[1]), bf16),
            pltpu.VMEM((tp_count, part, width), bf16),
            pltpu.VMEM((tp_count, part, width), bf16),
            pltpu.VMEM((part, width), f32),
            pltpu.VMEM((team * (halo + rows), width), bf16),
            pltpu.VMEM((2, halo + rows, piece), f32),
            pltpu.VMEM((rows, piece), bf16),
            pltpu.VMEM((team, 2, pairs * part, width), bf16),
            pltpu.VMEM((team, pairs * part, width), bf16),
            pltpu.VMEM((team, pairs, part, width), bf16),
            pltpu.VMEM((team, pairs, part, width), bf16),
            pltpu.VMEM((team, part, width), bf16),
            pltpu.VMEM((team, part, width), bf16),
            dma((10,)),
            dma((lines,)),
            dma((lines,)),
            dma((lines,)),
            dma((lines,)),
            dma((2, lines)),
            dma((2, lines)),
            dma((2, lines)),
            dma((2, lines)),
            dma((tp_count,)),
            dma((tp_count,)),
            dma((team, tp_count)),
            dma((team, tp_count)),
            dma((team,)),
            dma((team,)),
            dma((team,)),
            dma((team,)),
            dma((team, pairs)),
            dma((team, pairs)),
            dma((team,)),
            dma((team,)),
            dma((team,)),
            dma((team,)),
        ],
        compiler_params=pltpu.CompilerParams(
            collective_id=0, has_side_effects=True, vmem_limit_bytes=60 * 1024 * 1024
        ),
    )(*args)


def solution(mesh):
    in_specs = (
        P("sp", "tp"),
        P("sp", "tp"),
        P("sp", "tp"),
        P("sp", "tp"),
        P("sp", "tp"),
        P("tp"),
        P(),
        P("tp", None),
        P("sp", None),
        P(),
        P("sp", "tp"),
        P("sp", "tp"),
        P(None, "tp"),
        P(None, "tp"),
        P("tp", None),
    )
    body = functools.partial(shards, mesh.shape["sp"], mesh.shape["tp"])
    return jax.shard_map(
        body, mesh=mesh, in_specs=in_specs, out_specs=P(("sp", "tp"), None), check_vma=False
    )
```

time: 155 us -> 119 us (0.77)
  the two profiles are of different devices: /device:TPU:17 before, /device:TPU:10 now
where the time goes in v1:
time: 119 us
  Pallas kernels  117 us (98%)
  local copies, waits for them, and re-layouts  1.62 us (1%)
    pallas_call x1, Pallas kernels, shards(): pl.pallas_call(functools.partial(layer, sp_count, tp_count, team), out_sh...  117 us

profile of v1, /device:TPU:10, one launch (start us, length us, event | category | flops | bytes accessed | tf_op | source)
XLA Modules:
  0.0 118.8 jit_solution(11256666736040558776)
XLA Ops:
  0.0 117.2 %shard_map.145 = bf16[48,2048]{1,0:T(8,128)(2,1)} custom-call(bf16[192,128]{1,0:T(8,128)(2,1)} %q_a.1, bf16[192,128]{1,0:T(8,128)(2,1)} %k_a.1, bf16[192,128]{1,0:T(8,128)(2,1)} %q_b.1, bf16[192,128]{1,0:T(8,128)(2,1)} %k_b.1, bf16[192,256]{1,0:T(8,128)(2,1)} %vals.1, f32[2]{0:T(128)} %lambdas.1, f32[1,128]{1,0:T(1,128)} %bitcast.3, ...), custom_call_target="tpu_custom_call" | custom-call | tf_op jit(solution)/shard_map/pallas_call | solution.py:602
  117.2 1.6 %copy.17 = bf16[48,2048]{1,0:T(8,128)(2,1)} copy(bf16[48,2048]{1,0:T(8,128)(2,1)} %shard_map.145) | data formatting | bytes 393216

commit v2 on v1

--- a/solution.py
+++ b/solution.py
@@ -63,14 +63,17 @@
     kvz_recv,
     kvx_send,
     kvx_recv,
+    relay_send,
     wz_send,
     wz_recv,
     wx_send,
     wx_recv,
     rs_send,
     rs_recv,
-    ag_send,
-    ag_recv,
+    gy_send,
+    gy_recv,
+    gc_send,
+    gc_recv,
     halo_send,
     halo_recv,
     pair_send,
@@ -81,6 +84,7 @@
     z_recv,
     team_send,
     team_recv,
+    up_send,
 ):
     s = lax.axis_index("sp")
     t = lax.axis_index("tp")
@@ -103,6 +107,9 @@
     fresh = ff - (team - 1) * piece
     g = lax.rem(z, team)
     base = z - g
+    pairs = tp_count // 2
+    c_own = lax.rem(t, 2)
+    k_own = t // 2
     slot_rows = halo + rows
 
     def member(slot):
@@ -199,6 +206,16 @@
         block = kv_block(line * lanes + x)
         return remote(block, block, kvz_send.at[index], kvz_recv.at[line], to * lanes + x, t)
 
+    def kv_relay(line):
+        block = kv_block(line * lanes + x)
+        return remote(
+            block, block, relay_send.at[line], kvz_recv.at[line], (z + 1) * lanes + x, t
+        )
+
+    def relays(line):
+        direct = (line == z - 1) & (lax.rem(line, 2) == 0)
+        return (z + 1 < lines) & jnp.logical_not(direct)
+
     def kvx(line, lane):
         block = kv_block(line * lanes + lane)
         return remote(block, block, kvx_send.at[line], kvx_recv.at[line], mate, t)
@@ -217,10 +234,13 @@
     for load in kv_loads:
         load.wait()
 
-    @pl.loop(0, lines - 1 - z)
-    def _(i):
-        to = lines - 1 - i
-        kvz(z, to, to).start()
+    @pl.when((lax.rem(z, 2) == 0) & (z + 2 < lines))
+    def _():
+        kvz(z, z + 2, z + 2).start()
+
+    @pl.when(z + 1 < lines)
+    def _():
+        kvz(z, z + 1, z + 1).start()
 
     kvx(z, x).start()
     for load in w_loads:
@@ -240,9 +260,22 @@
 
         by_width(to, act)
 
+    def deferred(to):
+        return (to - z >= 2) & (lax.rem(to, team) == team - 1)
+
+    def send_first(to):
+        @pl.when(jnp.logical_not(deferred(to)))
+        def _():
+            send_weights(to)
+
+    def send_later(to):
+        @pl.when(deferred(to))
+        def _():
+            send_weights(to)
+
     @pl.loop(1, lines)
     def _(distance):
-        near(distance, send_weights)
+        near(distance, send_first)
 
     scale = head_dim**-0.5
     column = lax.broadcasted_iota(jnp.int32, (rows, key_width), 1) // head_dim
@@ -262,6 +295,11 @@
         def _():
             kvz(line - 1, mate // lanes, line - 1).wait_recv()
             kvx(line - 1, x).start()
+
+            @pl.when(relays(line - 1))
+            def _():
+                kv_relay(line - 1).start()
+
 
         @pl.when(i == jnp.maximum(z - 1, 0))
         def _():
@@ -322,8 +360,6 @@
         by_width(z, act)
 
     early = min(3, lines - 1)
-    if early > 0:
-        near(1, forward)
 
     out_load.wait()
     res_load.wait()
@@ -361,49 +397,116 @@
         rows_here = ffn.at[ffn_rows(slot, t)]
         return remote(rows_here, rows_here, team_send.at[to], team_recv.at[slot], member(to), t)
 
-    def gather_copy(i, slot, rank):
-        to = lax.rem(t + i, tp_count)
-        rows_here = ffn.at[ffn_rows(slot, rank)]
-        return remote(rows_here, rows_here, ag_send.at[slot, to], ag_recv.at[slot, rank], s, to)
-
-    for i in range(1, team):
-        team_copy(g, lax.rem(g + i, team)).start()
-    for i in range(1, tp_count):
-        gather_copy(i, g, t).start()
-    if early > 1:
-        near(2, forward)
-    for i in range(1, tp_count):
-        gather_copy(i, g, lax.rem(t + i, tp_count)).wait_recv()
-
-    after = lax.rem(s + 1, sp_count)
-    after_line = after // lanes
-    after_slot = lax.rem(after_line, team)
-    after_base = after_line - after_slot
-
-    def halo_copy(which, slot):
-        return remote(
-            ffn.at[pl.ds(pl.multiple_of(g * slot_rows + rows, 16), halo)],
-            ffn.at[pl.ds(pl.multiple_of(slot * slot_rows, 16), halo)],
-            halo_send.at[which],
-            halo_recv.at[slot],
-            (after_base + which) * lanes + lax.rem(after, lanes),
+    def relayed_up(slot, at_slot):
+        direct = (slot == at_slot - 1) & (lax.rem(slot, 2) == 0)
+        return (slot < at_slot) & (at_slot + 1 < team) & jnp.logical_not(direct)
+
+    def sent_direct(to):
+        return (to < g) | (to == g + 1) | ((to == g + 2) & (lax.rem(g, 2) == 0))
+
+    def team_relay(slot):
+        rows_here = ffn.at[ffn_rows(slot, t)]
+        return remote(
+            rows_here, rows_here, up_send.at[slot], team_recv.at[slot], member(g + 1), t
+        )
+
+    def y_gather(slot, k, source):
+        rows_here = ffn.at[ffn_rows(slot, 2 * source + c_own)]
+        return remote(
+            rows_here, rows_here, gy_send.at[slot, k], gy_recv.at[slot, source], s, 2 * k + c_own
+        )
+
+    def core_gather(slot, k, c):
+        rows_here = ffn.at[ffn_rows(slot, 2 * k + c)]
+        return remote(
+            rows_here, rows_here, gc_send.at[slot, k], gc_recv.at[slot, k], s, t + 1 - 2 * c_own
+        )
+
+    def hold(slot):
+        for i in range(1, pairs):
+            y_gather(slot, lax.rem(k_own + i, pairs), k_own).start()
+        core_gather(slot, k_own, c_own).start()
+
+    def halo_copy(slot, to_slot, to):
+        return remote(
+            ffn.at[pl.ds(pl.multiple_of(slot * slot_rows + rows, 16), halo)],
+            ffn.at[pl.ds(pl.multiple_of(to_slot * slot_rows, 16), halo)],
+            halo_send.at[slot],
+            halo_recv.at[to_slot],
+            to,
             t,
         )
 
-    @pl.when(s < sp_count - 1)
-    def _():
-        for which in range(team):
-            halo_copy(which, after_slot).start()
-
-    for slot in range(team):
-        if slot == team - 1 and early > 2:
+    def halos(slot, act):
+        @pl.when(x < lanes - 1)
+        def _():
+            act(halo_copy(slot, slot, mate))
+
+        @pl.when((x == lanes - 1) & (slot < team - 1))
+        def _():
+            act(halo_copy(slot, slot + 1, mate))
+
+        @pl.when((x == lanes - 1) & (slot == team - 1) & (z + team < lines))
+        def _():
+            act(halo_copy(slot, 0, (z + team) * lanes))
+
+    def pass_on(slot):
+        for i in range(1, pairs):
+            k = lax.rem(k_own + i, pairs)
+            y_gather(slot, k, k).wait_recv()
+            core_gather(slot, k, c_own).start()
+
+    def ready(slot):
+        for k in range(pairs):
+            core_gather(slot, k, 1 - c_own).wait_recv()
+        halos(slot, lambda copy: copy.start())
+
+    @pl.loop(0, team)
+    def _(i):
+        to = jnp.where(i < g, i, team - 1 - i + g)
+
+        @pl.when(sent_direct(to) & (to != g))
+        def _():
+            team_copy(g, to).start()
+
+    hold(g)
+
+    @pl.loop(1, lines)
+    def _(distance):
+        near(distance, send_later)
+
+    if early > 0:
+        near(1, forward)
+    pass_on(g)
+    ready(g)
+
+    def other(slot, act):
+        @pl.when(slot != g)
+        def _():
+            act(slot)
+
+    def take(slot):
+        team_copy(slot, g).wait_recv()
+
+        @pl.when(relayed_up(slot, g))
+        def _():
+            team_relay(slot).start()
+
+        hold(slot)
+
+    def settle(slot):
+        pass_on(slot)
+        ready(slot)
+
+    for slot in range(team + 1):
+        if slot == 2 and early > 1:
+            near(2, forward)
+        if slot == 3 and early > 2:
             near(3, forward)
-
-        @pl.when(slot != g)
-        def _():
-            team_copy(slot, g).wait_recv()
-            for i in range(1, tp_count):
-                gather_copy(i, slot, t).start()
+        if slot < team:
+            other(slot, take)
+        if slot > 0:
+            other(slot - 1, settle)
 
     @pl.loop(early + 1, lines)
     def _(distance):
@@ -418,12 +521,11 @@
         by_width(z, act)
 
     down_load.wait()
-    pairs = tp_count // 2
-    c_own = lax.rem(t, 2)
-    k_own = t // 2
     chunk = 512 if width % 512 == 0 else width
 
     def slot_of(n):
+        if team > 2 and n < 2:
+            n = jnp.where(g == team - 2, 1 - n, n)
         return lax.rem(g + 1 + n, team)
 
     def part_rows(k):
@@ -457,11 +559,6 @@
     def compute(n):
         slot = slot_of(n)
 
-        @pl.when(slot != g)
-        def _():
-            for i in range(1, tp_count):
-                gather_copy(i, slot, lax.rem(t + i, tp_count)).wait_recv()
-
         block = member(slot)
         halo_rows = pl.ds(pl.multiple_of(slot * slot_rows, 16), halo)
 
@@ -471,7 +568,7 @@
 
         @pl.when(block > 0)
         def _():
-            halo_copy(0, slot).wait_recv()
+            halo_copy(slot, slot, mate).wait_recv()
 
         rows_at = pl.ds(pl.multiple_of(slot * slot_rows, 16), slot_rows)
         for c in range(2):
@@ -536,9 +633,19 @@
         stream[...] += z_in[source].astype(f32)
     out[...] = stream[...].astype(bf16)
 
-    @pl.loop(z + 1, lines)
-    def _(to):
-        kvz(z, to, to).wait_send()
+    @pl.when((lax.rem(z, 2) == 0) & (z + 2 < lines))
+    def _():
+        kvz(z, z + 2, z + 2).wait_send()
+
+    @pl.when(z + 1 < lines)
+    def _():
+        kvz(z, z + 1, z + 1).wait_send()
+
+    @pl.loop(0, z)
+    def _(line):
+        @pl.when(relays(line))
+        def _():
+            kv_relay(line).wait_send()
 
     @pl.loop(0, z + 1)
     def _(line):
@@ -562,23 +669,29 @@
 
         by_width(z, act)
 
-    for i in range(1, team):
-        team_copy(g, lax.rem(g + i, team)).wait_send()
     for i in range(1, tp_count):
         part_copy(i).wait_send()
-        for slot in range(team):
-            gather_copy(i, slot, t).wait_send()
+    for slot in range(team):
+
+        @pl.when(sent_direct(slot) & (slot != g))
+        def _():
+            team_copy(g, slot).wait_send()
+
+        @pl.when(relayed_up(slot, g))
+        def _():
+            team_relay(slot).wait_send()
+
+        for i in range(1, pairs):
+            y_gather(slot, lax.rem(k_own + i, pairs), k_own).wait_send()
+        for k in range(pairs):
+            core_gather(slot, k, c_own).wait_send()
+        halos(slot, lambda copy: copy.wait_send())
     for n in range(team):
         pair_copy(n).wait_send()
         for i in range(1, pairs):
             y_copy(n, lax.rem(k_own + i, pairs), k_own).wait_send()
         if n < team - 1:
             z_copy(n, g).wait_send()
-
-    @pl.when(s < sp_count - 1)
-    def _():
-        for which in range(team):
-            halo_copy(which, after_slot).wait_send()
 
 
 def shards(sp_count, tp_count, *args):
@@ -629,20 +742,24 @@
             dma((lines,)),
             dma((lines,)),
             dma((lines,)),
+            dma((lines,)),
             dma((2, lines)),
             dma((2, lines)),
             dma((2, lines)),
             dma((2, lines)),
             dma((tp_count,)),
             dma((tp_count,)),
-            dma((team, tp_count)),
-            dma((team, tp_count)),
-            dma((team,)),
-            dma((team,)),
-            dma((team,)),
-            dma((team,)),
             dma((team, pairs)),
             dma((team, pairs)),
+            dma((team, pairs)),
+            dma((team, pairs)),
+            dma((team,)),
+            dma((team,)),
+            dma((team,)),
+            dma((team,)),
+            dma((team, pairs)),
+            dma((team, pairs)),
+            dma((team,)),
             dma((team,)),
             dma((team,)),
             dma((team,)),

time: 119 us -> 109 us (0.916)
  the two profiles are of different devices: /device:TPU:10 before, /device:TPU:17 now
where the time goes in v2:
time: 109 us; the launch traced here: 108 us
  Pallas kernels  107 us (98%)
  local copies, waits for them, and re-layouts  1.62 us (1%)
    pallas_call x1, Pallas kernels, shards(): pl.pallas_call(functools.partial(layer, sp_count, tp_count, team), out_sh...  107 us

profile of v2, /device:TPU:17, one launch (start us, length us, event | category | flops | bytes accessed | tf_op | source)
XLA Modules:
  0.0 108.3 jit_solution(9637304810778102626)
XLA Ops:
  0.0 106.6 %shard_map.145 = bf16[48,2048]{1,0:T(8,128)(2,1)} custom-call(bf16[192,128]{1,0:T(8,128)(2,1)} %q_a.1, bf16[192,128]{1,0:T(8,128)(2,1)} %k_a.1, bf16[192,128]{1,0:T(8,128)(2,1)} %q_b.1, bf16[192,128]{1,0:T(8,128)(2,1)} %k_b.1, bf16[192,256]{1,0:T(8,128)(2,1)} %vals.1, f32[2]{0:T(128)} %lambdas.1, f32[1,128]{1,0:T(1,128)} %bitcast.3, ...), custom_call_target="tpu_custom_call" | custom-call | tf_op jit(solution)/shard_map/pallas_call | solution.py:715
  106.7 1.6 %copy.17 = bf16[48,2048]{1,0:T(8,128)(2,1)} copy(bf16[48,2048]{1,0:T(8,128)(2,1)} %shard_map.145) | data formatting | bytes 393216

commit v3 on v2

--- a/solution.py
+++ b/solution.py
@@ -261,7 +261,11 @@
         by_width(to, act)
 
     def deferred(to):
-        return (to - z >= 2) & (lax.rem(to, team) == team - 1)
+        step = to - z
+        slot = lax.rem(to, team)
+        up = ((slot == team // 2) & (step <= 2)) | ((slot == team - 1) & (step == 1))
+        down = (step != -2) | (slot != 0)
+        return jnp.logical_not(jnp.where(step > 0, up, down))
 
     def send_first(to):
         @pl.when(jnp.logical_not(deferred(to)))
@@ -359,8 +363,6 @@
 
         by_width(z, act)
 
-    early = min(3, lines - 1)
-
     out_load.wait()
     res_load.wait()
     stream[...] = res[...].astype(f32)
@@ -397,17 +399,24 @@
         rows_here = ffn.at[ffn_rows(slot, t)]
         return remote(rows_here, rows_here, team_send.at[to], team_recv.at[slot], member(to), t)
 
-    def relayed_up(slot, at_slot):
-        direct = (slot == at_slot - 1) & (lax.rem(slot, 2) == 0)
-        return (slot < at_slot) & (at_slot + 1 < team) & jnp.logical_not(direct)
-
-    def sent_direct(to):
-        return (to < g) | (to == g + 1) | ((to == g + 2) & (lax.rem(g, 2) == 0))
-
-    def team_relay(slot):
+    def direct(source, to):
+        if team < 4:
+            return True
+        if source < to:
+            return to - source == 1 or (to - source == 2 and source % 2 == 0)
+        return (source, to) != (2, 0)
+
+    def relay_to(source, at):
+        if at > source and at + 1 < team and not direct(source, at + 1):
+            return at + 1
+        if at < source and at > 0 and not direct(source, at - 1):
+            return at - 1
+        return None
+
+    def team_relay(slot, to):
         rows_here = ffn.at[ffn_rows(slot, t)]
         return remote(
-            rows_here, rows_here, up_send.at[slot], team_recv.at[slot], member(g + 1), t
+            rows_here, rows_here, up_send.at[slot], team_recv.at[slot], member(to), t
         )
 
     def y_gather(slot, k, source):
@@ -461,56 +470,60 @@
             core_gather(slot, k, 1 - c_own).wait_recv()
         halos(slot, lambda copy: copy.start())
 
-    @pl.loop(0, team)
-    def _(i):
-        to = jnp.where(i < g, i, team - 1 - i + g)
-
-        @pl.when(sent_direct(to) & (to != g))
-        def _():
-            team_copy(g, to).start()
-
-    hold(g)
-
-    @pl.loop(1, lines)
-    def _(distance):
-        near(distance, send_later)
-
-    if early > 0:
-        near(1, forward)
-    pass_on(g)
-    ready(g)
-
-    def other(slot, act):
-        @pl.when(slot != g)
-        def _():
-            act(slot)
-
-    def take(slot):
-        team_copy(slot, g).wait_recv()
-
-        @pl.when(relayed_up(slot, g))
-        def _():
-            team_relay(slot).start()
-
+    targets = {(4, 0): (2, 1), (4, 1): (2, 0), (4, 2): (1, 3), (4, 3): (0, 1, 2)}
+    orders = {
+        (4, 0): "w1 o w3 x1 s1 x3 w2 x2 s3 s2",
+        (4, 1): "w2 w3 x0 x2 s0 o s2 w0 x3 s3",
+        (4, 2): "w3 w0 x0 w1 x1 o s0 s1 x3 s3",
+        (4, 3): "w2 x2 o w0 w1 x0 s2 x1 s0 s1",
+    }
+
+    def take(slot, at):
+        team_copy(slot, at).wait_recv()
+        to = relay_to(slot, at)
+        if to is not None:
+            team_relay(slot, to).start()
         hold(slot)
 
     def settle(slot):
         pass_on(slot)
         ready(slot)
 
-    for slot in range(team + 1):
-        if slot == 2 and early > 1:
-            near(2, forward)
-        if slot == 3 and early > 2:
-            near(3, forward)
-        if slot < team:
-            other(slot, take)
-        if slot > 0:
-            other(slot - 1, settle)
-
-    @pl.loop(early + 1, lines)
-    def _(distance):
-        near(distance, forward)
+    def plan(at):
+        others = [j for j in range(team) if j != at]
+        for to in targets.get((team, at), others):
+            team_copy(at, to).start()
+        hold(at)
+
+        @pl.loop(1, lines)
+        def _(i):
+            near(lines - i, send_later)
+
+        default = " ".join(["o"] + [kind + str(j) for kind in "wxs" for j in others])
+        for step in orders.get((team, at), default).split():
+            if step == "o":
+                settle(at)
+            elif step[0] == "w":
+                forward(base + int(step[1]))
+            elif step[0] == "x":
+                take(int(step[1]), at)
+            else:
+                settle(int(step[1]))
+
+    def at_own(act):
+        for at in range(team):
+
+            @pl.when(g == at)
+            def _():
+                act(at)
+
+    at_own(plan)
+
+    if lines > team:
+
+        @pl.loop(0, lines - team)
+        def _(i):
+            forward(jnp.where(i < base, i, i + team))
 
     @pl.loop(0, lines)
     def _(line):
@@ -523,10 +536,15 @@
     down_load.wait()
     chunk = 512 if width % 512 == 0 else width
 
+    turns = {4: ((2, 3, 1, 0), (2, 3, 0, 1), (0, 1, 3, 2), (0, 1, 2, 3))}
+
     def slot_of(n):
-        if team > 2 and n < 2:
-            n = jnp.where(g == team - 2, 1 - n, n)
-        return lax.rem(g + 1 + n, team)
+        if team not in turns:
+            return lax.rem(g + 1 + n, team)
+        slot = turns[team][0][n]
+        for at in range(1, team):
+            slot = jnp.where(g == at, turns[team][at][n], slot)
+        return slot
 
     def part_rows(k):
         return pl.ds(pl.multiple_of(k * part, 16), part)
@@ -620,13 +638,13 @@
         else:
             stream[...] += total
 
-    for n in range(team + 2):
+    for n in range(team + 1):
         if n < team:
             compute(n)
-        if 0 < n <= team:
+        if n > 0:
             across(n - 1)
-        if n > 1:
-            along(n - 2)
+    for n in range(team):
+        along(n)
     for n in range(team - 1):
         source = slot_of(n)
         z_copy(n, source).wait_recv()
@@ -671,16 +689,19 @@
 
     for i in range(1, tp_count):
         part_copy(i).wait_send()
+
+    def sent(at):
+        for slot in range(team):
+            if slot == at:
+                continue
+            if (team, at) not in targets or slot in targets[team, at]:
+                team_copy(at, slot).wait_send()
+            to = relay_to(slot, at)
+            if to is not None:
+                team_relay(slot, to).wait_send()
+
+    at_own(sent)
     for slot in range(team):
-
-        @pl.when(sent_direct(slot) & (slot != g))
-        def _():
-            team_copy(g, slot).wait_send()
-
-        @pl.when(relayed_up(slot, g))
-        def _():
-            team_relay(slot).wait_send()
-
         for i in range(1, pairs):
             y_gather(slot, lax.rem(k_own + i, pairs), k_own).wait_send()
         for k in range(pairs):

time: 109 us -> 99.1 us (0.909)
  the two profiles are of different devices: /device:TPU:17 before, /device:TPU:29 now
where the time goes in v3:
time: 99.1 us; the launch traced here: 98.9 us
  Pallas kernels  97.3 us (98%)
  local copies, waits for them, and re-layouts  1.62 us (2%)
    pallas_call x1, Pallas kernels, shards(): pl.pallas_call(functools.partial(layer, sp_count, tp_count, team), out_sh...  97.3 us

profile of v3, /device:TPU:29, one launch (start us, length us, event | category | flops | bytes accessed | tf_op | source)
XLA Modules:
  0.0 98.9 jit_solution(3545112017965466753)
XLA Ops:
  0.0 97.3 %shard_map.145 = bf16[48,2048]{1,0:T(8,128)(2,1)} custom-call(bf16[192,128]{1,0:T(8,128)(2,1)} %q_a.1, bf16[192,128]{1,0:T(8,128)(2,1)} %k_a.1, bf16[192,128]{1,0:T(8,128)(2,1)} %q_b.1, bf16[192,128]{1,0:T(8,128)(2,1)} %k_b.1, bf16[192,256]{1,0:T(8,128)(2,1)} %vals.1, f32[2]{0:T(128)} %lambdas.1, f32[1,128]{1,0:T(1,128)} %bitcast.3, ...), custom_call_target="tpu_custom_call" | custom-call | tf_op jit(solution)/shard_map/pallas_call | solution.py:736
  97.3 1.6 %copy.17 = bf16[48,2048]{1,0:T(8,128)(2,1)} copy(bf16[48,2048]{1,0:T(8,128)(2,1)} %shard_map.145) | data formatting | bytes 393216

commit v4 on v3

--- a/solution.py
+++ b/solution.py
@@ -253,29 +253,28 @@
             def _():
                 act(line)
 
-    def send_weights(to):
-        def act(skip):
-            for c in range(2):
-                wz(c, z, to, to, skip).start()
-
-        by_width(to, act)
-
-    def deferred(to):
+    def deferred(to, c):
         step = to - z
         slot = lax.rem(to, team)
         up = ((slot == team // 2) & (step <= 2)) | ((slot == team - 1) & (step == 1))
-        down = (step != -2) | (slot != 0)
+        down = (step != -2) | (slot != 0) | (c == 0)
         return jnp.logical_not(jnp.where(step > 0, up, down))
 
+    def send_weights(to, later):
+        def act(skip):
+            for c in range(2):
+
+                @pl.when(deferred(to, c) == later)
+                def _():
+                    wz(c, z, to, to, skip).start()
+
+        by_width(to, act)
+
     def send_first(to):
-        @pl.when(jnp.logical_not(deferred(to)))
-        def _():
-            send_weights(to)
+        send_weights(to, False)
 
     def send_later(to):
-        @pl.when(deferred(to))
-        def _():
-            send_weights(to)
+        send_weights(to, True)
 
     @pl.loop(1, lines)
     def _(distance):
@@ -292,17 +291,28 @@
     query_pos = s * rows + lax.broadcasted_iota(jnp.int32, (rows, span), 0)
     key_step = lax.broadcasted_iota(jnp.int32, (rows, span), 1)
 
+    hurry = (z >= 2) & (z + 1 < lines)
+
+    def take_keys(line):
+        kvz(line, mate // lanes, line).wait_recv()
+
+        @pl.when(relays(line))
+        def _():
+            kv_relay(line).start()
+
+        kvx(line, x).start()
+
+    @pl.when(hurry)
+    def _():
+        take_keys(z - 1)
+        take_keys(z - 2)
+
     def attend(i, state):
         line = z - i
 
-        @pl.when(i < z)
+        @pl.when((i < z) & ((i > 1) | jnp.logical_not(hurry)))
         def _():
-            kvz(line - 1, mate // lanes, line - 1).wait_recv()
-            kvx(line - 1, x).start()
-
-            @pl.when(relays(line - 1))
-            def _():
-                kv_relay(line - 1).start()
+            take_keys(line - 1)
 
 
         @pl.when(i == jnp.maximum(z - 1, 0))
@@ -355,9 +365,9 @@
         diff = sums_a / total_a - lambdas[h] * (sums_b / total_b)
         heads[:, h * value_dim : (h + 1) * value_dim] = rms_scale(diff, head_gain[...]).astype(bf16)
 
-    def forward(line):
+    def forward(line, parts=(0, 1)):
         def act(skip):
-            for c in range(2):
+            for c in parts:
                 wz(c, line, mate // lanes, line, skip).wait_recv()
                 wx(c, line, x, skip).start()
 
@@ -472,10 +482,10 @@
 
     targets = {(4, 0): (2, 1), (4, 1): (2, 0), (4, 2): (1, 3), (4, 3): (0, 1, 2)}
     orders = {
-        (4, 0): "w1 o w3 x1 s1 x3 w2 x2 s3 s2",
-        (4, 1): "w2 w3 x0 x2 s0 o s2 w0 x3 s3",
-        (4, 2): "w3 w0 x0 w1 x1 o s0 s1 x3 s3",
-        (4, 3): "w2 x2 o w0 w1 x0 s2 x1 s0 s1",
+        (4, 0): ("w1", "o", "w3", "x1", "a2", "s1", "x3", "b2", "x2", "s3", "s2"),
+        (4, 1): ("w2", "w3", "x0", "x2", "s0", "o", "s2", "w0", "x3", "s3"),
+        (4, 2): ("w3", "w0", "x0", "w1", "x1", "o", "s0", "s1", "x3", "s3"),
+        (4, 3): ("w2", "x2", "o", "w0", "w1", "x0", "s2", "x1", "s0", "s1"),
     }
 
     def take(slot, at):
@@ -499,12 +509,12 @@
         def _(i):
             near(lines - i, send_later)
 
-        default = " ".join(["o"] + [kind + str(j) for kind in "wxs" for j in others])
-        for step in orders.get((team, at), default).split():
+        default = ["o"] + [kind + str(j) for kind in "wxs" for j in others]
+        for step in orders.get((team, at), default):
             if step == "o":
                 settle(at)
-            elif step[0] == "w":
-                forward(base + int(step[1]))
+            elif step[0] in "wab":
+                forward(base + int(step[1]), {"w": (0, 1), "a": (0,), "b": (1,)}[step[0]])
             elif step[0] == "x":
                 take(int(step[1]), at)
             else:
@@ -534,7 +544,8 @@
         by_width(z, act)
 
     down_load.wait()
-    chunk = 512 if width % 512 == 0 else width
+    halves, half = pair_out.shape[1], pair_out.shape[4]
+    chunk = 512 if half % 512 == 0 else half
 
     turns = {4: ((2, 3, 1, 0), (2, 3, 0, 1), (0, 1, 3, 2), (0, 1, 2, 3))}
 
@@ -549,32 +560,32 @@
     def part_rows(k):
         return pl.ds(pl.multiple_of(k * part, 16), part)
 
-    def pair_copy(n):
+    def pair_copy(n, h):
         return remote(
-            pair_out.at[n, 1 - c_own],
-            pair_in.at[n],
-            pair_send.at[n],
-            pair_recv.at[n],
+            pair_out.at[n, h, 1 - c_own],
+            pair_in.at[n, h],
+            pair_send.at[n, h],
+            pair_recv.at[n, h],
             s,
             t + 1 - 2 * c_own,
         )
 
-    def y_copy(n, k, source):
+    def y_copy(n, h, k, source):
         return remote(
-            y_out.at[n, k],
-            y_in.at[n, source],
-            y_send.at[n, k],
-            y_recv.at[n, source],
+            y_out.at[n, h, k],
+            y_in.at[n, h, source],
+            y_send.at[n, h, k],
+            y_recv.at[n, h, source],
             s,
             2 * k + c_own,
         )
 
-    def z_copy(n, source):
+    def z_copy(n, h, kind, to):
         return remote(
-            z_out.at[n], z_in.at[source], z_send.at[n], z_recv.at[source], member(slot_of(n)), t
-        )
-
-    def compute(n):
+            z_out.at[n, h], z_in.at[kind, h], z_send.at[n, h], z_recv.at[kind, h], member(to), t
+        )
+
+    def front(n):
         slot = slot_of(n)
 
         block = member(slot)
@@ -607,49 +618,81 @@
             if (i + 1) * 128 <= piece - fresh:
                 value = jnp.where(g < team - 1, value, 0.0)
             hidden[:, at] = value.astype(bf16)
-        for i in range(width // chunk):
-            at = slice(i * chunk, (i + 1) * chunk)
-            product = jnp.dot(hidden[...], down[:, at], preferred_element_type=f32).astype(bf16)
-            for r in range(tp_count):
-                first = (r // 2) * part
-                pair_out[n, r % 2, first : first + part, at] = product[r * part : (r + 1) * part]
-        pair_copy(n).start()
-
-    def pair_sum(n, k):
-        mine = pair_out[n, c_own, part_rows(k), :].astype(f32)
-        return mine + pair_in[n, part_rows(k), :].astype(f32)
+
+    def back(n):
+        for h in range(halves):
+            for i in range(half // chunk):
+                at = slice(i * chunk, (i + 1) * chunk)
+                down_at = slice(h * half + i * chunk, h * half + (i + 1) * chunk)
+                product = jnp.dot(
+                    hidden[...], down[:, down_at], preferred_element_type=f32
+                ).astype(bf16)
+                for r in range(tp_count):
+                    first = (r // 2) * part
+                    pair_out[n, h, r % 2, first : first + part, at] = product[
+                        r * part : (r + 1) * part
+                    ]
+            pair_copy(n, h).start()
+
+    def pair_sum(n, h, k):
+        mine = pair_out[n, h, c_own, part_rows(k), :].astype(f32)
+        return mine + pair_in[n, h, part_rows(k), :].astype(f32)
 
     def across(n):
-        pair_copy(n).wait_recv()
+        for h in range(halves):
+            pair_copy(n, h).wait_recv()
+            for i in range(1, pairs):
+                k = lax.rem(k_own + i, pairs)
+                y_out[n, h, k] = pair_sum(n, h, k).astype(bf16)
+                y_copy(n, h, k, k_own).start()
+
+    far = 2 if team == 4 else 0
+    near_slot = g + 1 - 2 * lax.rem(g, 2)
+    inner = (g == 1) | (g == 2)
+
+    def along(n, h):
+        at = slice(h * half, (h + 1) * half)
+        total = pair_sum(n, h, k_own)
         for i in range(1, pairs):
             k = lax.rem(k_own + i, pairs)
-            y_out[n, k] = pair_sum(n, k).astype(bf16)
-            y_copy(n, k, k_own).start()
-
-    def along(n):
-        total = pair_sum(n, k_own)
-        for i in range(1, pairs):
-            k = lax.rem(k_own + i, pairs)
-            y_copy(n, k, k).wait_recv()
-            total = total + y_in[n, k].astype(f32)
-        if n < team - 1:
-            z_out[n] = total.astype(bf16)
-            z_copy(n, g).start()
+            y_copy(n, h, k, k).wait_recv()
+            total = total + y_in[n, h, k].astype(f32)
+        if n < far:
+
+            @pl.when(inner)
+            def _():
+                z_copy(n, h, 2 + n, near_slot).wait_recv()
+                z_out[n, h] = (total + z_in[2 + n, h].astype(f32)).astype(bf16)
+                z_copy(n, h, 1, slot_of(n)).start()
+
+            @pl.when(jnp.logical_not(inner))
+            def _():
+                z_out[n, h] = total.astype(bf16)
+                z_copy(n, h, 2 + n, near_slot).start()
+
+        elif n < team - 1:
+            z_out[n, h] = total.astype(bf16)
+            z_copy(n, h, 0, near_slot).start()
         else:
-            stream[...] += total
+            stream[:, at] += total
 
     for n in range(team + 1):
         if n < team:
-            compute(n)
+            front(n)
         if n > 0:
             across(n - 1)
+        if n < team:
+            back(n)
     for n in range(team):
-        along(n)
-    for n in range(team - 1):
-        source = slot_of(n)
-        z_copy(n, source).wait_recv()
-        stream[...] += z_in[source].astype(f32)
-    out[...] = stream[...].astype(bf16)
+        for h in range(halves):
+            along(n, h)
+    for h in range(halves):
+        at = slice(h * half, (h + 1) * half)
+        total = stream[:, at]
+        for kind in range(min(2, team - 1) if far else team - 1):
+            z_copy(0, h, kind, near_slot).wait_recv()
+            total = total + z_in[kind, h].astype(f32)
+        out[:, at] = total.astype(bf16)
 
     @pl.when((lax.rem(z, 2) == 0) & (z + 2 < lines))
     def _():
@@ -708,11 +751,12 @@
             core_gather(slot, k, c_own).wait_send()
         halos(slot, lambda copy: copy.wait_send())
     for n in range(team):
-        pair_copy(n).wait_send()
-        for i in range(1, pairs):
-            y_copy(n, lax.rem(k_own + i, pairs), k_own).wait_send()
-        if n < team - 1:
-            z_copy(n, g).wait_send()
+        for h in range(halves):
+            pair_copy(n, h).wait_send()
+            for i in range(1, pairs):
+                y_copy(n, h, lax.rem(k_own + i, pairs), k_own).wait_send()
+            if n < team - 1:
+                z_copy(n, h, 0, near_slot).wait_send()
 
 
 def shards(sp_count, tp_count, *args):
@@ -725,6 +769,8 @@
     team = next(n for n in (4, 2, 1) if lines % n == 0)
     pairs = tp_count // 2
     piece = -(-ff // (team * 128)) * 128
+    halves = 2 if width % 256 == 0 else 1
+    half = width // halves
     args = list(args)
     args[6] = head_gain.reshape(1, -1)
     args[9] = mix_gain.reshape(1, -1)
@@ -752,12 +798,12 @@
             pltpu.VMEM((team * (halo + rows), width), bf16),
             pltpu.VMEM((2, halo + rows, piece), f32),
             pltpu.VMEM((rows, piece), bf16),
-            pltpu.VMEM((team, 2, pairs * part, width), bf16),
-            pltpu.VMEM((team, pairs * part, width), bf16),
-            pltpu.VMEM((team, pairs, part, width), bf16),
-            pltpu.VMEM((team, pairs, part, width), bf16),
-            pltpu.VMEM((team, part, width), bf16),
-            pltpu.VMEM((team, part, width), bf16),
+            pltpu.VMEM((team, halves, 2, pairs * part, half), bf16),
+            pltpu.VMEM((team, halves, pairs * part, half), bf16),
+            pltpu.VMEM((team, halves, pairs, part, half), bf16),
+            pltpu.VMEM((team, halves, pairs, part, half), bf16),
+            pltpu.VMEM((team, halves, part, half), bf16),
+            pltpu.VMEM((4, halves, part, half), bf16),
             dma((10,)),
             dma((lines,)),
             dma((lines,)),
@@ -776,12 +822,12 @@
             dma((team, pairs)),
             dma((team,)),
             dma((team,)),
-            dma((team,)),
-            dma((team,)),
-            dma((team, pairs)),
-            dma((team, pairs)),
-            dma((team,)),
-            dma((team,)),
+            dma((team, halves)),
+            dma((team, halves)),
+            dma((team, halves, pairs)),
+            dma((team, halves, pairs)),
+            dma((team, halves)),
+            dma((4, halves)),
             dma((team,)),
             dma((team,)),
             dma((team,)),

time: 99.1 us -> 96 us (0.969)
  the two profiles are of different devices: /device:TPU:29 before, /device:TPU:17 now
where the time goes in v4:
time: 96 us; the launch traced here: 94.2 us
  Pallas kernels  92.6 us (96%)
  local copies, waits for them, and re-layouts  1.62 us (2%)
    pallas_call x1, Pallas kernels, shards(): pl.pallas_call(functools.partial(layer, sp_count, tp_count, team), out_sh...  92.6 us

profile of v4, /device:TPU:17, one launch (start us, length us, event | category | flops | bytes accessed | tf_op | source)
XLA Modules:
  0.0 94.2 jit_solution(11499605920217559472)
XLA Ops:
  0.0 92.6 %shard_map.145 = bf16[48,2048]{1,0:T(8,128)(2,1)} custom-call(bf16[192,128]{1,0:T(8,128)(2,1)} %q_a.1, bf16[192,128]{1,0:T(8,128)(2,1)} %k_a.1, bf16[192,128]{1,0:T(8,128)(2,1)} %q_b.1, bf16[192,128]{1,0:T(8,128)(2,1)} %k_b.1, bf16[192,256]{1,0:T(8,128)(2,1)} %vals.1, f32[2]{0:T(128)} %lambdas.1, f32[1,128]{1,0:T(1,128)} %bitcast.3, ...), custom_call_target="tpu_custom_call" | custom-call | tf_op jit(solution)/shard_map/pallas_call | solution.py:782
  92.6 1.6 %copy.17 = bf16[48,2048]{1,0:T(8,128)(2,1)} copy(bf16[48,2048]{1,0:T(8,128)(2,1)} %shard_map.145) | data formatting | bytes 393216

commit v5 on v4

--- a/solution.py
+++ b/solution.py
@@ -23,22 +23,22 @@
     sp_count,
     tp_count,
     team,
-    q_a,
+    q_a_in,
     k_a,
-    q_b,
+    q_b_in,
     k_b,
     vals,
     lambdas,
-    head_gain,
+    head_gain_in,
     out_weight,
     residual,
-    mix_gain,
+    mix_gain_in,
     gate_weight,
     up_weight,
-    gate_taps,
-    up_taps,
+    gate_taps_in,
+    up_taps_in,
     down_weight,
-    out,
+    result,
     kv,
     w_own,
     w,
@@ -58,6 +58,13 @@
     y_in,
     z_out,
     z_in,
+    q_a,
+    q_b,
+    head_gain,
+    mix_gain,
+    gate_taps,
+    up_taps,
+    out,
     local,
     kvz_send,
     kvz_recv,
@@ -101,6 +108,8 @@
     part = rows // tp_count
     width = out.shape[1]
     w_rows = gate_weight.shape[0]
+    w_parts = wz_recv.shape[2]
+    w_piece = w_rows // w_parts
     ff = gate_weight.shape[1]
     taps = gate_taps.shape[0]
     piece = w.shape[2]
@@ -111,6 +120,10 @@
     c_own = lax.rem(t, 2)
     k_own = t // 2
     slot_rows = halo + rows
+    kv_parts = kvz_recv.shape[1]
+    kv_piece = rows // kv_parts
+    row_parts = team_recv.shape[1]
+    row_piece = part // row_parts
 
     def member(slot):
         return (base + slot) * lanes + x
@@ -142,12 +155,55 @@
             device_id_type=pl.DeviceIdType.MESH,
         )
 
-    def kv_block(block):
+    def sent_all(block, sem):
+        remote(block, block, sem, sem, s, t).wait_send()
+
+    def came_all(block, sem):
+        remote(block, block, sem, sem, s, t).wait_recv()
+
+    def kv_rows(block):
         return kv.at[pl.ds(pl.multiple_of(block * rows, 16), rows)]
 
-    def w_block(c, block, skip=0):
-        at = pl.ds(pl.multiple_of(block * w_rows, 16), w_rows)
+    def kv_block(block, p):
+        return kv.at[pl.ds(pl.multiple_of(block * rows + p * kv_piece, 16), kv_piece)]
+
+    def w_block(c, block):
+        return w.at[c, pl.ds(pl.multiple_of(block * w_rows, 16), w_rows)]
+
+    def w_part(c, block, skip, p):
+        at = pl.ds(pl.multiple_of(block * w_rows + p * w_piece, 16), w_piece)
         return w.at[c, at, pl.ds(skip, piece - skip)]
+
+    barrier = pltpu.get_barrier_semaphore()
+
+    @pl.loop(1, sp_count)
+    def _(i):
+        pl.semaphore_signal(
+            barrier,
+            inc=1,
+            device_id=(lax.rem(s + i, sp_count), t),
+            device_id_type=pl.DeviceIdType.MESH,
+        )
+
+    @pl.loop(1, tp_count)
+    def _(i):
+        pl.semaphore_signal(
+            barrier,
+            inc=1,
+            device_id=(s, lax.rem(t + i, tp_count)),
+            device_id_type=pl.DeviceIdType.MESH,
+        )
+
+    @pl.loop(1, team)
+    def _(j):
+        @pl.loop(1, tp_count)
+        def _(i):
+            pl.semaphore_signal(
+                barrier,
+                inc=1,
+                device_id=(member(lax.rem(g + j, team)), lax.rem(t + i, tp_count)),
+                device_id_type=pl.DeviceIdType.MESH,
+            )
 
     own = pl.ds(pl.multiple_of(s * rows, 16), rows)
     kv_loads = (
@@ -166,83 +222,69 @@
         residual.at[pl.ds(pl.multiple_of(t * part, 16), part)], res, local.at[6]
     )
     down_load = pltpu.make_async_copy(down_weight.at[pl.ds(columns(z), piece)], down, local.at[7])
-    for load in kv_loads + w_loads + (out_load, res_load, down_load):
+    small_loads = (
+        pltpu.make_async_copy(q_a_in, q_a, local.at[10]),
+        pltpu.make_async_copy(q_b_in, q_b, local.at[11]),
+        pltpu.make_async_copy(head_gain_in, head_gain, local.at[12]),
+        pltpu.make_async_copy(mix_gain_in, mix_gain, local.at[13]),
+        pltpu.make_async_copy(gate_taps_in, gate_taps, local.at[14]),
+        pltpu.make_async_copy(up_taps_in, up_taps, local.at[15]),
+    )
+    for load in kv_loads + w_loads + small_loads + (out_load, res_load, down_load):
         load.start()
 
-    barrier = pltpu.get_barrier_semaphore()
-
-    @pl.loop(1, sp_count)
-    def _(i):
-        pl.semaphore_signal(
-            barrier,
-            inc=1,
-            device_id=(lax.rem(s + i, sp_count), t),
-            device_id_type=pl.DeviceIdType.MESH,
-        )
-
-    @pl.loop(1, tp_count)
-    def _(i):
-        pl.semaphore_signal(
-            barrier,
-            inc=1,
-            device_id=(s, lax.rem(t + i, tp_count)),
-            device_id_type=pl.DeviceIdType.MESH,
-        )
-
-    @pl.loop(1, team)
-    def _(j):
-        @pl.loop(1, tp_count)
-        def _(i):
-            pl.semaphore_signal(
-                barrier,
-                inc=1,
-                device_id=(member(lax.rem(g + j, team)), lax.rem(t + i, tp_count)),
-                device_id_type=pl.DeviceIdType.MESH,
-            )
-
     pl.semaphore_wait(barrier, sp_count - 1 + team * (tp_count - 1))
 
-    def kvz(line, to, index):
-        block = kv_block(line * lanes + x)
-        return remote(block, block, kvz_send.at[index], kvz_recv.at[line], to * lanes + x, t)
-
-    def kv_relay(line):
-        block = kv_block(line * lanes + x)
+    def kvz(line, to, p):
+        block = kv_block(line * lanes + x, p)
         return remote(
-            block, block, relay_send.at[line], kvz_recv.at[line], (z + 1) * lanes + x, t
+            block, block, kvz_send.at[to], kvz_recv.at[line, p], to * lanes + x, t
+        )
+
+    def kv_relay(line, p):
+        block = kv_block(line * lanes + x, p)
+        return remote(
+            block, block, relay_send.at[line], kvz_recv.at[line, p], (z + 1) * lanes + x, t
         )
 
     def relays(line):
         direct = (line == z - 1) & (lax.rem(line, 2) == 0)
         return (z + 1 < lines) & jnp.logical_not(direct)
 
-    def kvx(line, lane):
-        block = kv_block(line * lanes + lane)
+    def kvx(line, lane, p):
+        block = kv_block(line * lanes + lane, p)
         return remote(block, block, kvx_send.at[line], kvx_recv.at[line], mate, t)
 
-    def wz(c, line, to, index, skip):
-        block = w_block(c, line * lanes + x, skip)
+    def wz(c, line, to, skip, p):
         at = pl.ds(pl.multiple_of(columns(to) + skip, 128), piece - skip)
         return remote(
-            w_own.at[c, :, at], block, wz_send.at[c, index], wz_recv.at[c, line], to * lanes + x, t
-        )
-
-    def wx(c, line, lane, skip):
-        block = w_block(c, line * lanes + lane, skip)
-        return remote(block, block, wx_send.at[c, line], wx_recv.at[c, line], mate, t)
+            w_own.at[c, pl.ds(p * w_piece, w_piece), at],
+            w_part(c, line * lanes + x, skip, p),
+            wz_send.at[to],
+            wz_recv.at[c, line, p],
+            to * lanes + x,
+            t,
+        )
+
+    def wx(c, line, lane, skip, p):
+        block = w_part(c, line * lanes + lane, skip, p)
+        return remote(block, block, wx_send.at[0], wx_recv.at[0], mate, t)
 
     for load in kv_loads:
         load.wait()
 
     @pl.when((lax.rem(z, 2) == 0) & (z + 2 < lines))
     def _():
-        kvz(z, z + 2, z + 2).start()
+        for p in range(kv_parts):
+            kvz(z, z + 2, p).start()
 
     @pl.when(z + 1 < lines)
     def _():
-        kvz(z, z + 1, z + 1).start()
-
-    kvx(z, x).start()
+        for p in range(kv_parts):
+            kvz(z, z + 1, p).start()
+
+    for p in range(kv_parts):
+        kvx(z, x, p).start()
     for load in w_loads:
         load.wait()
 
@@ -256,7 +298,8 @@
     def deferred(to, c):
         step = to - z
         slot = lax.rem(to, team)
-        up = ((slot == team // 2) & (step <= 2)) | ((slot == team - 1) & (step == 1))
+        up = (slot == team // 2) & ((step == 2) | ((step == 1) & (c == 0)))
+        up = up | ((slot == team - 1) & (step == 1))
         down = (step != -2) | (slot != 0) | (c == 0)
         return jnp.logical_not(jnp.where(step > 0, up, down))
 
@@ -266,7 +309,8 @@
 
                 @pl.when(deferred(to, c) == later)
                 def _():
-                    wz(c, z, to, to, skip).start()
+                    for p in range(w_parts):
+                        wz(c, z, to, skip, p).start()
 
         by_width(to, act)
 
@@ -280,6 +324,8 @@
     def _(distance):
         near(distance, send_first)
 
+    for load in small_loads:
+        load.wait()
     scale = head_dim**-0.5
     column = lax.broadcasted_iota(jnp.int32, (rows, key_width), 1) // head_dim
     queries = [
@@ -294,13 +340,14 @@
     hurry = (z >= 2) & (z + 1 < lines)
 
     def take_keys(line):
-        kvz(line, mate // lanes, line).wait_recv()
-
-        @pl.when(relays(line))
-        def _():
-            kv_relay(line).start()
-
-        kvx(line, x).start()
+        for p in range(kv_parts):
+            kvz(line, mate // lanes, p).wait_recv()
+
+            @pl.when(relays(line))
+            def _():
+                kv_relay(line, p).start()
+
+            kvx(line, x, p).start()
 
     @pl.when(hurry)
     def _():
@@ -319,11 +366,12 @@
         def _():
             def act(skip):
                 for c in range(2):
-                    wx(c, z, x, skip).start()
+                    for p in range(w_parts):
+                        wx(c, z, x, skip, p).start()
 
             by_width(z, act)
 
-        kvx(line, 1 - x).wait_recv()
+        came_all(kv_rows(line * lanes + 1 - x), kvx_recv.at[line])
         keys_at = pl.ds(pl.multiple_of(line * span, 16), span)
         visible = line * span + key_step <= query_pos
         following = []
@@ -368,8 +416,9 @@
     def forward(line, parts=(0, 1)):
         def act(skip):
             for c in parts:
-                wz(c, line, mate // lanes, line, skip).wait_recv()
-                wx(c, line, x, skip).start()
+                for p in range(w_parts):
+                    wz(c, line, mate // lanes, skip, p).wait_recv()
+                    wx(c, line, x, skip, p).start()
 
         by_width(z, act)
 
@@ -377,26 +426,24 @@
     res_load.wait()
     stream[...] = res[...].astype(f32)
 
-    def part_copy(i):
-        to = lax.rem(t + i, tp_count)
-        return remote(part_out.at[to], part_in.at[t], rs_send.at[to], rs_recv.at[t], s, to)
-
-    for i in range(1, tp_count + 1):
-        to = lax.rem(t + i, tp_count)
-        product = jnp.dot(
-            heads[pl.ds(pl.multiple_of(to * part, 16), part), :],
-            out_w[...],
-            preferred_element_type=f32,
-        )
-        if i < tp_count:
-            part_out[to] = product.astype(bf16)
-            part_copy(i).start()
-        else:
-            stream[...] += product
-    for i in range(1, tp_count):
-        source = lax.rem(t + i, tp_count)
+    def part_copy(to):
+        return remote(part_out.at[to], part_in.at[t], rs_send.at[0], rs_recv.at[t], s, to)
+
+    def spread():
+        ranks = [2 * lax.rem(k_own + i, pairs) + c for i in range(1, pairs) for c in range(2)]
+        return ranks + [t + 1 - 2 * c_own]
+
+    def project_part(to):
+        at = pl.ds(pl.multiple_of(to * part, 16), part)
+        return jnp.dot(heads[at, :], out_w[...], preferred_element_type=f32)
+
+    for to in spread():
+        part_out[to] = project_part(to).astype(bf16)
+        part_copy(to).start()
+    stream[...] += project_part(t)
+    for source in reversed(spread()):
         remote(
-            part_out.at[source], part_in.at[source], rs_send.at[source], rs_recv.at[source], s, source
+            part_out.at[source], part_in.at[source], rs_send.at[0], rs_recv.at[source], s, source
         ).wait_recv()
         stream[...] += part_in[source].astype(f32)
 
@@ -405,9 +452,13 @@
 
     ffn[ffn_rows(g, t), :] = rms_scale(stream[...], mix_gain[...]).astype(bf16)
 
-    def team_copy(slot, to):
-        rows_here = ffn.at[ffn_rows(slot, t)]
-        return remote(rows_here, rows_here, team_send.at[to], team_recv.at[slot], member(to), t)
+    def row_block(slot, rank, p):
+        first = slot * slot_rows + halo + rank * part + p * row_piece
+        return ffn.at[pl.ds(pl.multiple_of(first, 16), row_piece)]
+
+    def team_copy(slot, to, p):
+        block = row_block(slot, t, p)
+        return remote(block, block, team_send.at[to], team_recv.at[slot, p], member(to), t)
 
     def direct(source, to):
         if team < 4:
@@ -423,28 +474,28 @@
             return at - 1
         return None
 
-    def team_relay(slot, to):
-        rows_here = ffn.at[ffn_rows(slot, t)]
+    def team_relay(slot, to, p):
+        block = row_block(slot, t, p)
+        return remote(block, block, up_send.at[slot], team_recv.at[slot, p], member(to), t)
+
+    def y_gather(slot, k, source, p):
+        block = row_block(slot, 2 * source + c_own, p)
         return remote(
-            rows_here, rows_here, up_send.at[slot], team_recv.at[slot], member(to), t
-        )
-
-    def y_gather(slot, k, source):
-        rows_here = ffn.at[ffn_rows(slot, 2 * source + c_own)]
-        return remote(
-            rows_here, rows_here, gy_send.at[slot, k], gy_recv.at[slot, source], s, 2 * k + c_own
+            block, block, gy_send.at[0], gy_recv.at[slot, source], s, 2 * k + c_own
         )
 
     def core_gather(slot, k, c):
         rows_here = ffn.at[ffn_rows(slot, 2 * k + c)]
         return remote(
-            rows_here, rows_here, gc_send.at[slot, k], gc_recv.at[slot, k], s, t + 1 - 2 * c_own
-        )
-
-    def hold(slot):
+            rows_here, rows_here, gc_send.at[0], gc_recv.at[slot], s, t + 1 - 2 * c_own
+        )
+
+    def some_rows(count):
+        return ffn.at[pl.ds(0, count * part)]
+
+    def hold(slot, p):
         for i in range(1, pairs):
-            y_gather(slot, lax.rem(k_own + i, pairs), k_own).start()
-        core_gather(slot, k_own, c_own).start()
+            y_gather(slot, lax.rem(k_own + i, pairs), k_own, p).start()
 
     def halo_copy(slot, to_slot, to):
         return remote(
@@ -472,28 +523,29 @@
     def pass_on(slot):
         for i in range(1, pairs):
             k = lax.rem(k_own + i, pairs)
-            y_gather(slot, k, k).wait_recv()
+            came_all(ffn.at[ffn_rows(slot, 2 * k + c_own)], gy_recv.at[slot, k])
             core_gather(slot, k, c_own).start()
 
     def ready(slot):
-        for k in range(pairs):
-            core_gather(slot, k, 1 - c_own).wait_recv()
+        came_all(some_rows(pairs), gc_recv.at[slot])
         halos(slot, lambda copy: copy.start())
 
     targets = {(4, 0): (2, 1), (4, 1): (2, 0), (4, 2): (1, 3), (4, 3): (0, 1, 2)}
     orders = {
         (4, 0): ("w1", "o", "w3", "x1", "a2", "s1", "x3", "b2", "x2", "s3", "s2"),
-        (4, 1): ("w2", "w3", "x0", "x2", "s0", "o", "s2", "w0", "x3", "s3"),
-        (4, 2): ("w3", "w0", "x0", "w1", "x1", "o", "s0", "s1", "x3", "s3"),
-        (4, 3): ("w2", "x2", "o", "w0", "w1", "x0", "s2", "x1", "s0", "s1"),
+        (4, 1): ("w2", "w3", "x0", "w0", "x2", "s0", "o", "x3", "s2", "s3"),
+        (4, 2): ("w3", "w0", "x0", "a1", "x1", "b1", "o", "s0", "s1", "x3", "s3"),
+        (4, 3): ("w2", "o", "x2", "w0", "w1", "x0", "x1", "s2", "s0", "s1"),
     }
 
     def take(slot, at):
-        team_copy(slot, at).wait_recv()
         to = relay_to(slot, at)
-        if to is not None:
-            team_relay(slot, to).start()
-        hold(slot)
+        for p in range(row_parts):
+            team_copy(slot, at, p).wait_recv()
+            if to is not None:
+                team_relay(slot, to, p).start()
+            hold(slot, p)
+        core_gather(slot, k_own, c_own).start()
 
     def settle(slot):
         pass_on(slot)
@@ -502,12 +554,15 @@
     def plan(at):
         others = [j for j in range(team) if j != at]
         for to in targets.get((team, at), others):
-            team_copy(at, to).start()
-        hold(at)
+            for p in range(row_parts):
+                team_copy(at, to, p).start()
+        for p in range(row_parts):
+            hold(at, p)
+        core_gather(at, k_own, c_own).start()
 
         @pl.loop(1, lines)
-        def _(i):
-            near(lines - i, send_later)
+        def _(distance):
+            near(distance, send_later)
 
         default = ["o"] + [kind + str(j) for kind in "wxs" for j in others]
         for step in orders.get((team, at), default):
@@ -535,13 +590,10 @@
         def _(i):
             forward(jnp.where(i < base, i, i + team))
 
-    @pl.loop(0, lines)
-    def _(line):
-        def act(skip):
-            for c in range(2):
-                wx(c, line, 1 - x, skip).wait_recv()
-
-        by_width(z, act)
+    def w_lines(skip):
+        return w.at[:, pl.ds(0, lines * w_rows), pl.ds(skip, piece - skip)]
+
+    by_width(z, lambda skip: came_all(w_lines(skip), wx_recv.at[0]))
 
     down_load.wait()
     halves, half = pair_out.shape[1], pair_out.shape[4]
@@ -564,7 +616,7 @@
         return remote(
             pair_out.at[n, h, 1 - c_own],
             pair_in.at[n, h],
-            pair_send.at[n, h],
+            pair_send.at[0],
             pair_recv.at[n, h],
             s,
             t + 1 - 2 * c_own,
@@ -574,15 +626,15 @@
         return remote(
             y_out.at[n, h, k],
             y_in.at[n, h, source],
-            y_send.at[n, h, k],
-            y_recv.at[n, h, source],
+            y_send.at[0],
+            y_recv.at[n, h, lax.rem(source - k + pairs - 1 + pairs, pairs)],
             s,
             2 * k + c_own,
         )
 
     def z_copy(n, h, kind, to):
         return remote(
-            z_out.at[n, h], z_in.at[kind, h], z_send.at[n, h], z_recv.at[kind, h], member(to), t
+            z_out.at[n, h], z_in.at[kind, h], z_send.at[0], z_recv.at[kind, h], member(to), t
         )
 
     def front(n):
@@ -650,26 +702,20 @@
     near_slot = g + 1 - 2 * lax.rem(g, 2)
     inner = (g == 1) | (g == 2)
 
-    def along(n, h):
+    def along(n, h, merging):
         at = slice(h * half, (h + 1) * half)
         total = pair_sum(n, h, k_own)
         for i in range(1, pairs):
             k = lax.rem(k_own + i, pairs)
-            y_copy(n, h, k, k).wait_recv()
+            y_copy(n, h, k_own, k).wait_recv()
             total = total + y_in[n, h, k].astype(f32)
-        if n < far:
-
-            @pl.when(inner)
-            def _():
-                z_copy(n, h, 2 + n, near_slot).wait_recv()
-                z_out[n, h] = (total + z_in[2 + n, h].astype(f32)).astype(bf16)
-                z_copy(n, h, 1, slot_of(n)).start()
-
-            @pl.when(jnp.logical_not(inner))
-            def _():
-                z_out[n, h] = total.astype(bf16)
-                z_copy(n, h, 2 + n, near_slot).start()
-
+        if n < far and merging:
+            z_copy(n, h, 2 + n, near_slot).wait_recv()
+            z_out[n, h] = (total + z_in[2 + n, h].astype(f32)).astype(bf16)
+            z_copy(n, h, 1, slot_of(n)).start()
+        elif n < far:
+            z_out[n, h] = total.astype(bf16)
+            z_copy(n, h, 2 + n, near_slot).start()
         elif n < team - 1:
             z_out[n, h] = total.astype(bf16)
             z_copy(n, h, 0, near_slot).start()
@@ -681,11 +727,91 @@
             front(n)
         if n > 0:
             across(n - 1)
+        if far and n == team - 1:
+
+            @pl.when(jnp.logical_not(inner))
+            def _():
+                for h in range(halves):
+                    along(0, h, False)
+
         if n < team:
             back(n)
-    for n in range(team):
-        for h in range(halves):
-            along(n, h)
+    @pl.when((lax.rem(z, 2) == 0) & (z + 2 < lines))
+    def _():
+        sent_all(kv_rows(s), kvz_send.at[z + 2])
+
+    @pl.when(z + 1 < lines)
+    def _():
+        sent_all(kv_rows(s), kvz_send.at[z + 1])
+
+    @pl.loop(0, z)
+    def _(line):
+        @pl.when(relays(line))
+        def _():
+            sent_all(kv_rows(s), relay_send.at[line])
+
+    @pl.loop(0, z + 1)
+    def _(line):
+        sent_all(kv_rows(s), kvx_send.at[line])
+
+    @pl.loop(1, lines)
+    def _(i):
+        to = lax.rem(z + i, lines)
+
+        def act(skip):
+            at = pl.ds(pl.multiple_of(columns(to) + skip, 128), piece - skip)
+            sent_all(w_own.at[:, :, at], wz_send.at[to])
+
+        by_width(to, act)
+
+    by_width(z, lambda skip: sent_all(w_lines(skip), wx_send.at[0]))
+
+    sent_all(part_out.at[pl.ds(0, tp_count - 1)], rs_send.at[0])
+
+    def sent(at):
+        for slot in range(team):
+            if slot == at:
+                continue
+            if (team, at) not in targets or slot in targets[team, at]:
+                sent_all(some_rows(1), team_send.at[slot])
+            to = relay_to(slot, at)
+            if to is not None:
+                sent_all(some_rows(1), up_send.at[slot])
+
+    at_own(sent)
+    for slot in range(team):
+        halos(slot, lambda copy: copy.wait_send())
+    sent_all(some_rows(team * (pairs - 1)), gy_send.at[0])
+    sent_all(some_rows(team * pairs), gc_send.at[0])
+    def leave(h):
+        at = pl.ds(h * half, half)
+        return pltpu.make_async_copy(out.at[:, at], result.at[:, at], local.at[16 + h])
+
+    def finish(merging):
+        rest = [(n, h) for n in range(1 if far else 0, team) for h in range(halves)]
+        if merging:
+            pairwise = [(n, h) for h in range(halves) for n in (1, 2)]
+            rest = [(0, h) for h in range(halves)] + pairwise + rest[2 * halves :]
+        for n, h in rest:
+            along(n, h, merging)
+
+    if far:
+
+        @pl.when(inner)
+        def _():
+            finish(True)
+
+        @pl.when(jnp.logical_not(inner))
+        def _():
+            finish(False)
+
+    else:
+        finish(False)
+    sent_all(pair_in, pair_send.at[0])
+    if pairs > 1:
+        sent_all(y_in.at[:, :, pl.ds(0, pairs - 1)], y_send.at[0])
+    if team > 1:
+        sent_all(z_out.at[pl.ds(0, team - 1)], z_send.at[0])
     for h in range(halves):
         at = slice(h * half, (h + 1) * half)
         total = stream[:, at]
@@ -693,70 +819,9 @@
             z_copy(0, h, kind, near_slot).wait_recv()
             total = total + z_in[kind, h].astype(f32)
         out[:, at] = total.astype(bf16)
-
-    @pl.when((lax.rem(z, 2) == 0) & (z + 2 < lines))
-    def _():
-        kvz(z, z + 2, z + 2).wait_send()
-
-    @pl.when(z + 1 < lines)
-    def _():
-        kvz(z, z + 1, z + 1).wait_send()
-
-    @pl.loop(0, z)
-    def _(line):
-        @pl.when(relays(line))
-        def _():
-            kv_relay(line).wait_send()
-
-    @pl.loop(0, z + 1)
-    def _(line):
-        kvx(line, x).wait_send()
-
-    @pl.loop(1, lines)
-    def _(i):
-        to = lax.rem(z + i, lines)
-
-        def act(skip):
-            for c in range(2):
-                wz(c, z, to, to, skip).wait_send()
-
-        by_width(to, act)
-
-    @pl.loop(0, lines)
-    def _(line):
-        def act(skip):
-            for c in range(2):
-                wx(c, line, x, skip).wait_send()
-
-        by_width(z, act)
-
-    for i in range(1, tp_count):
-        part_copy(i).wait_send()
-
-    def sent(at):
-        for slot in range(team):
-            if slot == at:
-                continue
-            if (team, at) not in targets or slot in targets[team, at]:
-                team_copy(at, slot).wait_send()
-            to = relay_to(slot, at)
-            if to is not None:
-                team_relay(slot, to).wait_send()
-
-    at_own(sent)
-    for slot in range(team):
-        for i in range(1, pairs):
-            y_gather(slot, lax.rem(k_own + i, pairs), k_own).wait_send()
-        for k in range(pairs):
-            core_gather(slot, k, c_own).wait_send()
-        halos(slot, lambda copy: copy.wait_send())
-    for n in range(team):
-        for h in range(halves):
-            pair_copy(n, h).wait_send()
-            for i in range(1, pairs):
-                y_copy(n, h, lax.rem(k_own + i, pairs), k_own).wait_send()
-            if n < team - 1:
-                z_copy(n, h, 0, near_slot).wait_send()
+        leave(h).start()
+    for h in range(halves):
+        leave(h).wait()
 
 
 def shards(sp_count, tp_count, *args):
@@ -769,21 +834,23 @@
     team = next(n for n in (4, 2, 1) if lines % n == 0)
     pairs = tp_count // 2
     piece = -(-ff // (team * 128)) * 128
-    halves = 2 if width % 256 == 0 else 1
+    halves = 4 if width % 512 == 0 else 1
+    kv_parts = 2 if rows % 32 == 0 else 1
+    w_parts = 2 if w_rows % 32 == 0 else 1
+    row_parts = part // 16 if part % 16 == 0 else 1
     half = width // halves
     args = list(args)
     args[6] = head_gain.reshape(1, -1)
     args[9] = mix_gain.reshape(1, -1)
-    vmem = pl.BlockSpec(memory_space=pltpu.VMEM)
     hbm = pl.BlockSpec(memory_space=pl.ANY)
     smem = pl.BlockSpec(memory_space=pltpu.SMEM)
     dma = pltpu.SemaphoreType.DMA
-    in_specs = [vmem, hbm, vmem, hbm, hbm, smem, vmem, hbm, hbm, vmem, hbm, hbm, vmem, vmem, hbm]
+    in_specs = [hbm] * 5 + [smem] + [hbm] * 9
     return pl.pallas_call(
         functools.partial(layer, sp_count, tp_count, team),
         out_shape=jax.ShapeDtypeStruct((part, width), bf16),
         in_specs=in_specs,
-        out_specs=vmem,
+        out_specs=hbm,
         scratch_shapes=[
             pltpu.VMEM((sp_count * rows, 2 * q_a.shape[1] + vals.shape[1]), bf16),
             pltpu.VMEM((2, w_rows, ff), bf16),
@@ -804,32 +871,39 @@
             pltpu.VMEM((team, halves, pairs, part, half), bf16),
             pltpu.VMEM((team, halves, part, half), bf16),
             pltpu.VMEM((4, halves, part, half), bf16),
-            dma((10,)),
+            pltpu.VMEM(q_a.shape, bf16),
+            pltpu.VMEM(q_a.shape, bf16),
+            pltpu.VMEM(args[6].shape, f32),
+            pltpu.VMEM(args[9].shape, f32),
+            pltpu.VMEM(args[12].shape, f32),
+            pltpu.VMEM(args[12].shape, f32),
+            pltpu.VMEM((part, width), bf16),
+            dma((16 + halves,)),
+            dma((lines,)),
+            dma((lines, kv_parts)),
             dma((lines,)),
             dma((lines,)),
             dma((lines,)),
             dma((lines,)),
-            dma((lines,)),
-            dma((2, lines)),
-            dma((2, lines)),
-            dma((2, lines)),
-            dma((2, lines)),
+            dma((2, lines, w_parts)),
+            dma((1,)),
+            dma((1,)),
+            dma((1,)),
             dma((tp_count,)),
-            dma((tp_count,)),
+            dma((1,)),
             dma((team, pairs)),
-            dma((team, pairs)),
-            dma((team, pairs)),
-            dma((team, pairs)),
+            dma((1,)),
             dma((team,)),
             dma((team,)),
+            dma((team,)),
+            dma((1,)),
             dma((team, halves)),
-            dma((team, halves)),
-            dma((team, halves, pairs)),
-            dma((team, halves, pairs)),
-            dma((team, halves)),
+            dma((1,)),
+            dma((team, halves, max(pairs - 1, 1))),
+            dma((1,)),
             dma((4, halves)),
             dma((team,)),
-            dma((team,)),
+            dma((team, row_parts)),
             dma((team,)),
         ],
         compiler_params=pltpu.CompilerParams(

time: 96 us -> 92.5 us (0.964)
  the two profiles are of different devices: /device:TPU:17 before, /device:TPU:27 now
where the time goes in v5:
time: 92.5 us; the launch traced here: 92.3 us
  Pallas kernels  90.7 us (98%)
  local copies, waits for them, and re-layouts  1.62 us (2%)
    pallas_call x1, Pallas kernels, shards(): pl.pallas_call(functools.partial(layer, sp_count, tp_count, team), out_sh...  90.7 us

profile of v5, /device:TPU:27, one launch (start us, length us, event | category | flops | bytes accessed | tf_op | source)
XLA Modules:
  0.0 92.3 jit_solution(17748813387920152186)
XLA Ops:
  0.0 90.7 %shard_map.145 = bf16[48,2048]{1,0:T(8,128)(2,1)} custom-call(bf16[192,128]{1,0:T(8,128)(2,1)} %q_a_in.1, bf16[192,128]{1,0:T(8,128)(2,1)} %k_a.1, bf16[192,128]{1,0:T(8,128)(2,1)} %q_b_in.1, bf16[192,128]{1,0:T(8,128)(2,1)} %k_b.1, bf16[192,256]{1,0:T(8,128)(2,1)} %vals.1, f32[2]{0:T(128)} %lambdas.1, f32[1,128]{1,0:T(1,128)} %bitcast.3, ...), custom_call_target="tpu_custom_call" | custom-call | tf_op jit(solution)/shard_map/pallas_call | solution.py:849
  90.7 1.6 %copy.17 = bf16[48,2048]{1,0:T(8,128)(2,1)} copy(bf16[48,2048]{1,0:T(8,128)(2,1)} %shard_map.145) | data formatting | bytes 393216

commit v6 on v5

--- a/solution.py
+++ b/solution.py
@@ -299,8 +299,8 @@
         step = to - z
         slot = lax.rem(to, team)
         up = (slot == team // 2) & ((step == 2) | ((step == 1) & (c == 0)))
-        up = up | ((slot == team - 1) & (step == 1))
-        down = (step != -2) | (slot != 0) | (c == 0)
+        up = up | (slot == team - 1)
+        down = (step != -1) | (slot != team // 2 - 1) | (c == 0)
         return jnp.logical_not(jnp.where(step > 0, up, down))
 
     def send_weights(to, later):
@@ -320,9 +320,22 @@
     def send_later(to):
         send_weights(to, True)
 
+    for distance in (3, 1, 2):
+
+        @pl.when(z >= distance)
+        def _():
+            send_first(z - distance)
+
     @pl.loop(1, lines)
     def _(distance):
-        near(distance, send_first)
+        @pl.when(z + distance < lines)
+        def _():
+            send_first(z + distance)
+
+        @pl.when((distance > 3) & (z >= distance))
+        def _():
+            send_first(z - distance)
+
 
     for load in small_loads:
         load.wait()
@@ -422,6 +435,16 @@
 
         by_width(z, act)
 
+    if team == 4:
+
+        @pl.when(g == 2)
+        def _():
+            forward(z + 1)
+
+        @pl.when(g == 3)
+        def _():
+            forward(z - 1)
+
     out_load.wait()
     res_load.wait()
     stream[...] = res[...].astype(f32)
@@ -532,10 +555,10 @@
 
     targets = {(4, 0): (2, 1), (4, 1): (2, 0), (4, 2): (1, 3), (4, 3): (0, 1, 2)}
     orders = {
-        (4, 0): ("w1", "o", "w3", "x1", "a2", "s1", "x3", "b2", "x2", "s3", "s2"),
-        (4, 1): ("w2", "w3", "x0", "w0", "x2", "s0", "o", "x3", "s2", "s3"),
-        (4, 2): ("w3", "w0", "x0", "a1", "x1", "b1", "o", "s0", "s1", "x3", "s3"),
-        (4, 3): ("w2", "o", "x2", "w0", "w1", "x0", "x1", "s2", "s0", "s1"),
+        (4, 0): ("w1", "w3", "o", "w2", "x1", "x2", "s1", "x3", "s2", "s3"),
+        (4, 1): ("w3", "x0", "a2", "x2", "w0", "s0", "o", "x3", "b2", "s2", "s3"),
+        (4, 2): ("w0", "x0", "a1", "x1", "o", "s0", "s1", "b1", "x3", "s3"),
+        (4, 3): ("w0", "o", "x2", "w1", "x0", "x1", "s2", "s0", "s1"),
     }
 
     def take(slot, at):

time: 92.5 us -> 89.9 us (0.972)
  the two profiles are of different devices: /device:TPU:27 before, /device:TPU:17 now
where the time goes in v6:
time: 89.9 us; the launch traced here: 88.9 us
  Pallas kernels  87.2 us (97%)
  local copies, waits for them, and re-layouts  1.62 us (2%)
    pallas_call x1, Pallas kernels, shards(): pl.pallas_call(functools.partial(layer, sp_count, tp_count, team), out_sh...  87.2 us

profile of v6, /device:TPU:17, one launch (start us, length us, event | category | flops | bytes accessed | tf_op | source)
XLA Modules:
  0.0 88.9 jit_solution(131046716462029582)
XLA Ops:
  0.0 87.2 %shard_map.145 = bf16[48,2048]{1,0:T(8,128)(2,1)} custom-call(bf16[192,128]{1,0:T(8,128)(2,1)} %q_a_in.1, bf16[192,128]{1,0:T(8,128)(2,1)} %k_a.1, bf16[192,128]{1,0:T(8,128)(2,1)} %q_b_in.1, bf16[192,128]{1,0:T(8,128)(2,1)} %k_b.1, bf16[192,256]{1,0:T(8,128)(2,1)} %vals.1, f32[2]{0:T(128)} %lambdas.1, f32[1,128]{1,0:T(1,128)} %bitcast.3, ...), custom_call_target="tpu_custom_call" | custom-call | tf_op jit(solution)/shard_map/pallas_call | solution.py:872
  87.2 1.6 %copy.17 = bf16[48,2048]{1,0:T(8,128)(2,1)} copy(bf16[48,2048]{1,0:T(8,128)(2,1)} %shard_map.145) | data formatting | bytes 393216

commit v7 on v6

--- a/solution.py
+++ b/solution.py
@@ -622,7 +622,7 @@
     halves, half = pair_out.shape[1], pair_out.shape[4]
     chunk = 512 if half % 512 == 0 else half
 
-    turns = {4: ((2, 3, 1, 0), (2, 3, 0, 1), (0, 1, 3, 2), (0, 1, 2, 3))}
+    turns = {4: ((2, 3, 1, 0), (0, 2, 3, 1), (3, 0, 1, 2), (0, 1, 2, 3))}
 
     def slot_of(n):
         if team not in turns:
@@ -732,11 +732,11 @@
             k = lax.rem(k_own + i, pairs)
             y_copy(n, h, k_own, k).wait_recv()
             total = total + y_in[n, h, k].astype(f32)
-        if n < far and merging:
-            z_copy(n, h, 2 + n, near_slot).wait_recv()
-            z_out[n, h] = (total + z_in[2 + n, h].astype(f32)).astype(bf16)
+        if merging and n in (1, 2):
+            z_copy(n, h, 1 + n, near_slot).wait_recv()
+            z_out[n, h] = (total + z_in[1 + n, h].astype(f32)).astype(bf16)
             z_copy(n, h, 1, slot_of(n)).start()
-        elif n < far:
+        elif n < far and not merging:
             z_out[n, h] = total.astype(bf16)
             z_copy(n, h, 2 + n, near_slot).start()
         elif n < team - 1:
@@ -751,6 +751,11 @@
         if n > 0:
             across(n - 1)
         if far and n == team - 1:
+
+            @pl.when(inner)
+            def _():
+                for h in range(halves):
+                    along(0, h, True)
 
             @pl.when(jnp.logical_not(inner))
             def _():
@@ -812,9 +817,6 @@
 
     def finish(merging):
         rest = [(n, h) for n in range(1 if far else 0, team) for h in range(halves)]
-        if merging:
-            pairwise = [(n, h) for h in range(halves) for n in (1, 2)]
-            rest = [(0, h) for h in range(halves)] + pairwise + rest[2 * halves :]
         for n, h in rest:
             along(n, h, merging)
 

time: 89.9 us -> 88.2 us (0.981)
  Pallas kernels: 87.2 us -> 86.1 us
    pallas_call x1, Pallas kernels: 87.2 us -> 86.1 us  [shards(): pl.pallas_call(functools.partial(layer, sp_count, tp_count, team), out_sh...]
where the time goes in v7:
time: 88.2 us; the launch traced here: 87.7 us
  Pallas kernels  86.1 us (98%)
  local copies, waits for them, and re-layouts  1.62 us (2%)
    pallas_call x1, Pallas kernels, shards(): pl.pallas_call(functools.partial(layer, sp_count, tp_count, team), out_sh...  86.1 us

profile of v7, /device:TPU:17, one launch (start us, length us, event | category | flops | bytes accessed | tf_op | source)
XLA Modules:
  0.0 87.7 jit_solution(9636279722122693726)
XLA Ops:
  0.0 86.1 %shard_map.145 = bf16[48,2048]{1,0:T(8,128)(2,1)} custom-call(bf16[192,128]{1,0:T(8,128)(2,1)} %q_a_in.1, bf16[192,128]{1,0:T(8,128)(2,1)} %k_a.1, bf16[192,128]{1,0:T(8,128)(2,1)} %q_b_in.1, bf16[192,128]{1,0:T(8,128)(2,1)} %k_b.1, bf16[192,256]{1,0:T(8,128)(2,1)} %vals.1, f32[2]{0:T(128)} %lambdas.1, f32[1,128]{1,0:T(1,128)} %bitcast.3, ...), custom_call_target="tpu_custom_call" | custom-call | tf_op jit(solution)/shard_map/pallas_call | solution.py:874
  86.1 1.6 %copy.17 = bf16[48,2048]{1,0:T(8,128)(2,1)} copy(bf16[48,2048]{1,0:T(8,128)(2,1)} %shard_map.145) | data formatting | bytes 393216
